TPU v7x, 256 devices: a whole 4x4x8 slice. The times are simulated.
256 devices in a mesh: sp: 128 (over z, y, x), tp: 2 (over core).
Axes of the slice: x: 4, y: 4, z: 8, core: 2. Of those that a mesh axis runs over, the one named last changes fastest.
Arguments:
- hidden: bfloat16 [32768, 2048], P('sp', 'tp'), may hold values from -16 to 16
- query_weight: bfloat16 [2048, 1024], P(None, 'tp'), may hold values from -0.125 to 0.125
- key_weight: bfloat16 [2048, 512], P(None, 'tp'), may hold values from -0.125 to 0.125
- value_weight: bfloat16 [2048, 512], P(None, 'tp'), may hold values from -0.125 to 0.125
- head_gate_weight: bfloat16 [2048, 1024], P(None, 'tp'), may hold values from -0.125 to 0.125
- state_in_weight: bfloat16 [2048, 1024], P(None, 'tp'), may hold values from -0.125 to 0.125
- state_gate_weight: bfloat16 [2048, 1024], P(None, 'tp'), may hold values from -0.125 to 0.125
- sink_logit: float32 [16], P('tp'), may hold values from 1 to 6
- decay_real: float32 [64, 64], P('tp'), may hold values from -0.7 to -0.0049
- decay_frequency: float32 [64, 64], P('tp'), may hold values from 0 to 192
- log_step: float32 [64], P('tp'), may hold values from -20 to 0
- input_real: float32 [64, 64, 16], P('tp'), may hold values from -8196 to 8196
- input_imaginary: float32 [64, 64, 16], P('tp'), may hold values from -8196 to 8196
- output_real: float32 [64, 16, 64], P('tp'), may hold values from -0.5 to 0.5
- output_imaginary: float32 [64, 16, 64], P('tp'), may hold values from -0.5 to 0.5
- skip_weight: float32 [64, 16], P('tp'), may hold values from -3 to 3
- decay_shift: float32 [64, 32768], P('tp', 'sp'), may hold values from -2 to 0
- head_out_weight: bfloat16 [1024, 2048], P('tp'), may hold values from -0.375 to 0.375
- state_out_weight: bfloat16 [1024, 2048], P('tp'), may hold values from -0.375 to 0.375
Outputs:
- layer_out: bfloat16 [32768, 2048], P('sp', 'tp')
All inputs are finite; a program needn't handle non-finite values.
Results may differ from a plain program's by a relative error of at most 0.012.
Values may be sent and summed in bfloat16 or wider, within the bound.
A program may use at most 128 MiB of HBM per device.

v0:
```python
import jax
import jax.numpy as jnp
from jax import lax
from jax.sharding import Mesh
from jax.sharding import PartitionSpec as P

HEAD_DIM = 64
Q_HEADS = 16
KV_HEADS = 8
GROUP_CH = 16
WINDOW = 128
SP = ("sp_0", "sp_1", "sp_2")


NEG_FILL = -1e30


def shifted(value, axis, steps):
    count = lax.axis_size(axis)
    first, last = (max(0, -steps), min(count, count - steps))
    return lax.ppermute(value, axis, [(source, source + steps) for source in range(first, last)])


def filled_with(x, identity):
    return jax.tree.map(
        lambda part, zero: jnp.zeros_like(part) + jnp.asarray(zero, part.dtype), x, identity
    )


def prefix_by_axis(x, axes, combine, identity):
    before = start = filled_with(x, identity)
    running = x
    for axis in reversed(axes):
        devices, mine = (lax.axis_size(axis), lax.axis_index(axis))
        pieces = jax.tree.map(lambda part: lax.all_gather(part, axis), running)
        inside, running = (start, start)
        for k in range(devices):
            passed = k < mine
            running = combine(running, jax.tree.map(lambda part: part[k], pieces))
            inside = jax.tree.map(lambda new, old: jnp.where(passed, new, old), running, inside)
        before = combine(inside, before)
    return before


def combine(earlier_pair, later_pair):
    prior_real, prior_imag, prior_sum_real, prior_sum_imag = earlier_pair
    after_real, after_imag, after_sum_real, after_sum_imag = later_pair
    return (
        prior_real * after_real - prior_imag * after_imag,
        prior_real * after_imag + prior_imag * after_real,
        after_real * prior_sum_real - after_imag * prior_sum_imag + after_sum_real,
        after_real * prior_sum_imag + after_imag * prior_sum_real + after_sum_imag,
    )


def within_segments(rows, segment, tile_width):
    extent = rows.shape[-1]
    leading = rows.shape[:-1]
    row_index = jnp.arange(tile_width, dtype=jnp.int32)[:, None]
    column_index = jnp.arange(tile_width, dtype=jnp.int32)[None, :]
    triangle = (
        (row_index // segment == column_index // segment) & (row_index <= column_index)
    ).astype(jnp.float32)
    flattened = rows.reshape(-1, tile_width)
    summed = jnp.dot(flattened, triangle)
    return summed.reshape(leading + (extent,))


def attend(query_rows_all, key_value, sink_logit, head_gate):
    tok_rows = query_rows_all.shape[0]
    kv_width = key_value.shape[1] // 2
    kv_heads = kv_width // HEAD_DIM
    group_size = Q_HEADS // KV_HEADS
    blocks = tok_rows // WINDOW
    previous = shifted(key_value[tok_rows - WINDOW :], SP, 1)
    joined = jnp.concatenate([previous, key_value], axis=0).reshape(
        blocks + 1, WINDOW, 2 * kv_width
    )
    banded = jnp.concatenate([joined[:-1], joined[1:]], axis=1)
    key_band = banded[..., :kv_width].reshape(blocks, 2 * WINDOW, kv_heads, HEAD_DIM)
    value_band = banded[..., kv_width:].reshape(blocks, 2 * WINDOW, kv_heads, HEAD_DIM)
    query_heads = query_rows_all.reshape(blocks, WINDOW, kv_heads, group_size, HEAD_DIM)
    scores = jnp.einsum(
        "nqkgd,nskd->nkgqs", query_heads, key_band, preferred_element_type=jnp.float32
    ) * HEAD_DIM ** (-0.5)
    query_index = jnp.arange(WINDOW, dtype=jnp.int32)[:, None]
    column = jnp.arange(2 * WINDOW, dtype=jnp.int32)[None, :]
    distance = WINDOW + query_index - column
    block_start = (
        lax.axis_index(SP) * tok_rows + jnp.arange(blocks, dtype=jnp.int32)[:, None, None] * WINDOW
    )
    allowed = (distance >= 0) & (distance < WINDOW) & (block_start - WINDOW + column >= 0)
    scores = jnp.where(allowed[:, None, None], scores, NEG_FILL)
    sink_col = sink_logit.reshape(kv_heads, group_size)[None, :, :, None, None]
    maxima = jnp.maximum(jnp.max(scores, axis=-1, keepdims=True), sink_col)
    exponent = jnp.exp(scores - maxima)
    totals = jnp.sum(exponent, axis=-1, keepdims=True) + jnp.exp(sink_col - maxima)
    weights = (exponent / totals).astype(jnp.bfloat16)
    attended = jnp.einsum(
        "nkgqs,nskd->nqkgd", weights, value_band, preferred_element_type=jnp.float32
    ).reshape(tok_rows, -1)
    return (jax.nn.sigmoid(head_gate.astype(jnp.float32)) * attended).astype(jnp.bfloat16)


def recur(
    state_input,
    state_gate,
    decay_real,
    decay_frequency,
    log_step,
    input_real,
    input_imaginary,
    output_real,
    output_imaginary,
    skip_weight,
    decay_shift,
):
    tok_rows = state_input.shape[0]
    groups = decay_real.shape[0]
    states = decay_real.shape[1]
    segment = min(16, tok_rows)
    tile_width = min(128, tok_rows)
    segment_count = tok_rows // segment
    stepsize = jnp.exp(log_step)[:, None]
    log_magnitude = decay_real * stepsize
    rotation = decay_frequency * stepsize
    magnitude = jnp.exp(log_magnitude)
    base_real = magnitude * jnp.cos(rotation)
    base_imag = magnitude * jnp.sin(rotation)
    denominator = decay_real * decay_real + decay_frequency * decay_frequency
    less_real = base_real - 1.0
    zoh_real = (less_real * decay_real + base_imag * decay_frequency) / denominator
    zoh_imag = (base_imag * decay_real - less_real * decay_frequency) / denominator
    drive_real = zoh_real[..., None] * input_real - zoh_imag[..., None] * input_imaginary
    drive_imag = zoh_real[..., None] * input_imaginary + zoh_imag[..., None] * input_real
    values = state_input.astype(jnp.float32).reshape(tok_rows, groups, GROUP_CH)
    push_real = jnp.einsum("tgp,gnp->gnt", values, drive_real)
    push_imag = jnp.einsum("tgp,gnp->gnt", values, drive_imag)
    counter = jnp.arange(1, segment + 1, dtype=jnp.float32)
    log_rate = counter * log_magnitude[..., None]
    angle_table = counter * rotation[..., None]
    repeats = (1, 1, segment_count)
    grow_rows = jnp.tile(jnp.exp(log_rate), repeats)
    shrink_rows = jnp.tile(jnp.exp(-log_rate), repeats)
    cosine = jnp.tile(jnp.cos(angle_table), repeats)
    sine_rows = jnp.tile(jnp.sin(angle_table), repeats)
    shift_sum = within_segments(decay_shift, segment, tile_width)
    inverse = jnp.exp(-shift_sum)[:, None, :] * shrink_rows
    weighted = jnp.stack(
        [
            inverse * (push_real * cosine + push_imag * sine_rows),
            inverse * (push_imag * cosine - push_real * sine_rows),
        ]
    )
    scaled = within_segments(weighted, segment, tile_width)
    grow = jnp.exp(shift_sum)[:, None, :] * grow_rows
    cum_real = grow * cosine
    cum_imag = grow * sine_rows
    local_real = cum_real * scaled[0] - cum_imag * scaled[1]
    local_imag = cum_real * scaled[1] + cum_imag * scaled[0]
    last = segment - 1
    segment_ends = (
        cum_real[..., last::segment],
        cum_imag[..., last::segment],
        local_real[..., last::segment],
        local_imag[..., last::segment],
    )
    inclusive = lax.associative_scan(combine, segment_ends, axis=2)
    summary = (
        inclusive[0][..., -1],
        inclusive[1][..., -1],
        inclusive[2][..., -1],
        inclusive[3][..., -1],
    )
    unity = jnp.ones_like(summary[0])
    nothing = jnp.zeros_like(summary[0])
    prefix = prefix_by_axis(summary, SP, combine, (unity, nothing, nothing, nothing))
    carry_real, carry_imag = (prefix[2], prefix[3])
    ones_col = jnp.ones((groups, states, 1), jnp.float32)
    zero_col = jnp.zeros((groups, states, 1), jnp.float32)
    before_cum_real = jnp.concatenate([ones_col, inclusive[0][..., :-1]], axis=2)
    before_cum_imag = jnp.concatenate([zero_col, inclusive[1][..., :-1]], axis=2)
    before_real = jnp.concatenate([zero_col, inclusive[2][..., :-1]], axis=2)
    before_imag = jnp.concatenate([zero_col, inclusive[3][..., :-1]], axis=2)
    entry_real = (
        before_real
        + before_cum_real * carry_real[..., None]
        - before_cum_imag * carry_imag[..., None]
    )
    entry_imag = (
        before_imag
        + before_cum_real * carry_imag[..., None]
        + before_cum_imag * carry_real[..., None]
    )
    entry_real_rows = jnp.repeat(entry_real, segment, axis=2)
    entry_imag_rows = jnp.repeat(entry_imag, segment, axis=2)
    state_real = local_real + cum_real * entry_real_rows - cum_imag * entry_imag_rows
    state_imag = local_imag + cum_real * entry_imag_rows + cum_imag * entry_real_rows
    recurrent = (
        jnp.einsum("gpn,gnt->tgp", output_real, state_real)
        - jnp.einsum("gpn,gnt->tgp", output_imaginary, state_imag)
        + skip_weight[None] * values
    )
    recurrent = recurrent.reshape(tok_rows, groups * GROUP_CH)
    return (jax.nn.sigmoid(state_gate.astype(jnp.float32)) * jax.nn.gelu(recurrent)).astype(
        jnp.bfloat16
    )


def on_device(
    hidden,
    query_weight,
    key_weight,
    value_weight,
    head_gate_weight,
    state_in_weight,
    state_gate_weight,
    sink_logit,
    decay_real,
    decay_frequency,
    log_step,
    input_real,
    input_imaginary,
    output_real,
    output_imaginary,
    skip_weight,
    decay_shift,
    head_out_weight,
    state_out_weight,
):
    weight_list = (
        query_weight,
        key_weight,
        value_weight,
        head_gate_weight,
        state_in_weight,
        state_gate_weight,
    )
    portion = lax.all_gather(hidden, "tp", axis=1, tiled=True)
    sums = tuple(
        (jnp.dot(portion, weight, preferred_element_type=jnp.float32) for weight in weight_list)
    )
    query_rows_all, key_rows, value_rows, head_gate, state_input, state_gate = tuple(
        (running.astype(jnp.bfloat16) for running in sums)
    )
    key_value = jnp.concatenate([key_rows, value_rows], axis=1)
    head_mixed = attend(query_rows_all, key_value, sink_logit, head_gate)
    state_mixed = recur(
        state_input,
        state_gate,
        decay_real,
        decay_frequency,
        log_step,
        input_real,
        input_imaginary,
        output_real,
        output_imaginary,
        skip_weight,
        decay_shift,
    )
    head_columns, state_columns = (
        lax.all_to_all(head_out_weight, "tp", split_axis=1, concat_axis=0, tiled=True),
        lax.all_to_all(state_out_weight, "tp", split_axis=1, concat_axis=0, tiled=True),
    )
    layer_out = jnp.dot(
        lax.all_gather(head_mixed, "tp", axis=1, tiled=True),
        head_columns,
        preferred_element_type=jnp.float32,
    ) + jnp.dot(
        lax.all_gather(state_mixed, "tp", axis=1, tiled=True),
        state_columns,
        preferred_element_type=jnp.float32,
    )
    return layer_out.astype(jnp.bfloat16)


def solution(mesh):
    split = Mesh(mesh.devices.reshape(8, 4, 4, mesh.shape["tp"]), ("sp_0", "sp_1", "sp_2", "tp"))
    in_specs = (
        P(SP, "tp"),
        P(None, "tp"),
        P(None, "tp"),
        P(None, "tp"),
        P(None, "tp"),
        P(None, "tp"),
        P(None, "tp"),
        P("tp"),
        P("tp", None),
        P("tp", None),
        P("tp"),
        P("tp", None, None),
        P("tp", None, None),
        P("tp", None, None),
        P("tp", None, None),
        P("tp", None),
        P("tp", SP),
        P("tp", None),
        P("tp", None),
    )
    out_specs = P(SP, "tp")
    return jax.shard_map(
        on_device, mesh=split, in_specs=in_specs, out_specs=out_specs, check_vma=False
    )
```

profile of v0, /device:TPU:225, one launch (start us, length us, event | category | flops | bytes accessed | tf_op | source)
XLA Modules:
  0.0 421.4 jit_solution(2638394154341600606)
XLA Ops:
  7.3 4.0 copy.325
  11.2 5.6 %all-to-all-start = ((bf16[512,2,1024]{0,2,1:T(8,128)(2,1)}), bf16[512,2,1024]{0,2,1:T(8,128)(2,1)}, u32[]{:S(2)}, u32[]{:S(2)}) async-start(bf16[512,2,1024]{0,2,1:T(8,128)(2,1)} %bitcast.1078), calls=%async_computation | async-start | bytes 4194304 | tf_op jit(solution)/shard_map/all_to_all | solution.py:262
  17.0 1.0 multiply_exponential_fusion
  18.0 2.3 tile.18
  20.4 4.1 copy.329
  24.4 2.3 tile.42
  26.7 3.9 copy.330
  30.6 2.3 tile.40
  32.9 3.9 copy.327
  38.5 3.9 copy.361
  42.4 5.0 %all-to-all-start.1 = ((bf16[512,2,1024]{0,2,1:T(8,128)(2,1)}), bf16[512,2,1024]{0,2,1:T(8,128)(2,1)}, u32[]{:S(2)}, u32[]{:S(2)}) async-start(bf16[512,2,1024]{0,2,1:T(8,128)(2,1)} %bitcast.1079), calls=%async_computation.1 | async-start | bytes 4194304 | tf_op jit(solution)/shard_map/all_to_all | solution.py:263
  47.4 4.0 copy.326
  51.4 4.0 copy.362
  56.3 2.7 convolution_convert_fusion
  58.9 1.2 copy.328
  60.2 1.5 fusion.33
  61.7 3.3 multiply_bitcast_fusion.1
  65.0 1.5 pad_maximum_fusion
  66.5 2.7 reshape.1225
  70.0 2.2 fusion.129
  72.2 1.9 squeeze.188
  74.1 2.8 copy.333
  76.9 1.9 squeeze.189
  78.8 2.7 copy.334
  81.5 9.7 %multiply_add_fusion = (f32[32,64,256]{1,2,0:T(8,128)}, f32[32,64,256]{1,2,0:T(8,128)}, f32[32,64,256]{1,2,0:T(8,128)}, f32[32,64,256]{1,2,0:T(8,128)}) fusion(f32[32,64,256]{1,2,0:T(8,128)} %copy.333, f32[32,64,256]{1,2,0:T(8,128)} %copy.334, f32[32,64,16]{1,2,0:T(8,128)S(1)} %get-tuple-element.108, f32[32,64,16]{1,2,0:T(8,128)S(1)} %get-tuple-element.109, ...), kind=kLoop, calls=%fused_computation.12 | loop fusion | flops 4718592 | bytes 13008896 | tf_op jit(solution)/shard_map/add | solution.py:160
  91.2 2.9 slice.485
  94.3 2.9 slice.493
  97.4 2.9 slice.487
  100.5 2.9 slice.491
  104.2 1.0 multiply_subtract_fusion.3
  114.5 1.0 subtract_add_fusion
  116.5 10.2 %pad.134 = f32[32,64,16]{1,2,0:T(8,128)} pad(f32[32,64,8]{1,2,0:T(8,128)S(1)} %pad_maximum_fusion.7, f32[]{:T(128)} %constant.81.clone.1), padding=0_0_0x0_0_0x0_1_1 | pad | bytes 196612 | tf_op jit(solution)/shard_map/pad | solution.py:168
  129.1 1.0 multiply_add_fusion.12
  134.7 10.3 %pad.290 = f32[32,64,15]{1,2,0:T(8,128)} pad(f32[32,64,8]{1,2,0:T(8,128)S(1)} %add.1142, f32[]{:T(128)} %constant.81.clone.1), padding=0_0_0x0_0_0x0_0_1 | pad | bytes 188420
  145.3 10.3 %pad.132 = f32[32,64,16]{1,2,0:T(8,128)} pad(f32[32,64,8]{1,2,0:T(8,128)S(1)} %pad_maximum_fusion.6, f32[]{:T(128)} %constant.81.clone.1), padding=0_0_0x0_0_0x0_1_1 | pad | bytes 196612 | tf_op jit(solution)/shard_map/pad | solution.py:168
  156.4 10.3 %pad.288 = f32[32,64,15]{1,2,0:T(8,128)} pad(f32[32,64,8]{1,2,0:T(8,128)S(1)} %add.1130, f32[]{:T(128)} %constant.81.clone.1), padding=0_0_0x0_0_0x0_0_1 | pad | bytes 188420
  168.2 9.5 %all-gather.3 = f32[128,64,1]{1,2,0:T(1,128)S(1)} all-gather(f32[32,64,1]{1,2,0:T(1,128)S(1)} %slice_add_fusion.20), channel_id=5, replica_groups=mesh['sp_0'=8,'sp_1'=4,'sp_2'=4,'tp'=2] {'sp_2'}, dimensions={0}, use_global_device_ids=true | all-gather | bytes 40960 | tf_op jit(solution)/shard_map/all_gather | solution.py:35
  178.9 9.0 %all-gather.1 = f32[128,64,1]{1,2,0:T(1,128)S(1)} all-gather(f32[32,64,1]{1,2,0:T(1,128)S(1)} %slice_add_fusion.21), channel_id=3, replica_groups=mesh['sp_0'=8,'sp_1'=4,'sp_2'=4,'tp'=2] {'sp_2'}, dimensions={0}, use_global_device_ids=true | all-gather | bytes 40960 | tf_op jit(solution)/shard_map/all_gather | solution.py:35
  188.8 9.0 %all-gather = f32[128,64,1]{1,2,0:T(1,128)S(1)} all-gather(f32[32,64,1]{1,2,0:T(1,128)S(1)} %slice.1580), channel_id=2, replica_groups=mesh['sp_0'=8,'sp_1'=4,'sp_2'=4,'tp'=2] {'sp_2'}, dimensions={0}, use_global_device_ids=true | all-gather | bytes 40960 | tf_op jit(solution)/shard_map/all_gather | solution.py:35
  198.7 9.0 %all-gather.2 = f32[128,64,1]{1,2,0:T(1,128)S(1)} all-gather(f32[32,64,1]{1,2,0:T(1,128)S(1)} %slice.1578), channel_id=4, replica_groups=mesh['sp_0'=8,'sp_1'=4,'sp_2'=4,'tp'=2] {'sp_2'}, dimensions={0}, use_global_device_ids=true | all-gather | bytes 40960 | tf_op jit(solution)/shard_map/all_gather | solution.py:35
  207.8 9.5 %all_gather.58 = f32[4,32,64]{2,1,0:T(8,128)S(1)} all-gather(f32[1,32,64]{2,1,0:T(8,128)S(1)} %fusion.105), channel_id=1, replica_groups=mesh['sp_0'=8,'sp_1'=4,'sp_2'=4,'tp'=2] {'sp_1'}, dimensions={0}, use_global_device_ids=true | all-gather | bytes 40960 | tf_op jit(solution)/shard_map/all_gather | solution.py:35
  217.3 9.0 %all_gather.57 = f32[4,32,64]{2,1,0:T(8,128)S(1)} all-gather(f32[1,32,64]{2,1,0:T(8,128)S(1)} %get-tuple-element.22), channel_id=1, replica_groups=mesh['sp_0'=8,'sp_1'=4,'sp_2'=4,'tp'=2] {'sp_1'}, dimensions={0}, use_global_device_ids=true | all-gather | bytes 40960 | tf_op jit(solution)/shard_map/all_gather | solution.py:35
  226.3 9.6 %all_gather.63 = f32[4,32,64]{2,1,0:T(8,128)S(1)} all-gather(f32[1,32,64]{2,1,0:T(8,128)S(1)} %get-tuple-element.76), channel_id=1, replica_groups=mesh['sp_0'=8,'sp_1'=4,'sp_2'=4,'tp'=2] {'sp_1'}, dimensions={0}, use_global_device_ids=true | all-gather | bytes 40960 | tf_op jit(solution)/shard_map/all_gather | solution.py:35
  235.9 9.0 %all_gather.64 = f32[4,32,64]{2,1,0:T(8,128)S(1)} all-gather(f32[1,32,64]{2,1,0:T(8,128)S(1)} %get-tuple-element.25), channel_id=1, replica_groups=mesh['sp_0'=8,'sp_1'=4,'sp_2'=4,'tp'=2] {'sp_1'}, dimensions={0}, use_global_device_ids=true | all-gather | bytes 40960 | tf_op jit(solution)/shard_map/all_gather | solution.py:35
  244.9 20.2 %all_gather.59 = f32[8,32,64]{2,1,0:T(8,128)} all-gather(f32[1,32,64]{2,1,0:T(8,128)S(1)} %get-tuple-element.70), channel_id=1, replica_groups=mesh['sp_0'=8,'sp_1'=4,'sp_2'=4,'tp'=2] {'sp_0'}, dimensions={0}, use_global_device_ids=true | all-gather | bytes 73728 | tf_op jit(solution)/shard_map/all_gather | solution.py:35
  265.2 20.5 %all_gather.65 = f32[8,32,64]{2,1,0:T(8,128)} all-gather(f32[1,32,64]{2,1,0:T(8,128)S(1)} %get-tuple-element.71), channel_id=1, replica_groups=mesh['sp_0'=8,'sp_1'=4,'sp_2'=4,'tp'=2] {'sp_0'}, dimensions={0}, use_global_device_ids=true | all-gather | bytes 73728 | tf_op jit(solution)/shard_map/all_gather | solution.py:35
  285.7 20.6 %all_gather.60 = f32[8,32,64]{2,1,0:T(8,128)} all-gather(f32[1,32,64]{2,1,0:T(8,128)S(1)} %get-tuple-element.16), channel_id=1, replica_groups=mesh['sp_0'=8,'sp_1'=4,'sp_2'=4,'tp'=2] {'sp_0'}, dimensions={0}, use_global_device_ids=true | all-gather | bytes 73728 | tf_op jit(solution)/shard_map/all_gather | solution.py:35
  306.3 20.2 %all_gather.66 = f32[8,32,64]{2,1,0:T(8,128)} all-gather(f32[1,32,64]{2,1,0:T(8,128)S(1)} %get-tuple-element.72), channel_id=1, replica_groups=mesh['sp_0'=8,'sp_1'=4,'sp_2'=4,'tp'=2] {'sp_0'}, dimensions={0}, use_global_device_ids=true | all-gather | bytes 73728 | tf_op jit(solution)/shard_map/all_gather | solution.py:35
  327.9 1.3 add_add_fusion.6
  330.2 4.5 %fusion.2 = (bf16[32,64,256]{1,2,0:T(8,128)(2,1)S(1)}, bf16[32,64,256]{1,2,0:T(8,128)(2,1)S(1)}) fusion(f32[32,64,256]{1,2,0:T(8,128)S(1)} %copy-done.2, f32[32,64,16]{1,2,0:T(8,128)S(1)} %get-tuple-element.41, f32[32,64,16]{1,2,0:T(8,128)S(1)} %get-tuple-element.40, f32[32,64,16]{1,2,0:T(8,128)S(1)} %get-tuple-element.108, ...), kind=kLoop, calls=%fused_computation.6 | loop fusion | flops 6815744 | bytes 6979584 | tf_op jit(solution)/shard_map/add | solution.py:198
  335.7 1.5 fusion.9
  337.2 1.4 copy.360
  338.6 2.2 convolution_convert_fusion.4
  341.3 2.2 collective-permute-start
  344.3 1.1 reshape.1316
  345.4 2.4 fusion.23
  347.8 50.1 %all_gather.67 = bf16[256,1024]{1,0:T(8,128)(2,1)} all-gather(bf16[256,512]{1,0:T(8,128)(2,1)S(1)} %fusion.23), channel_id=1, replica_groups=mesh['sp_0'=8,'sp_1'=4,'sp_2'=4,'tp'=2] {'tp'}, dimensions={1}, use_global_device_ids=true | all-gather | bytes 786432 | tf_op jit(solution)/shard_map/all_gather | solution.py:270
  399.1 1.6 fusion.131
  401.2 1.3 convolution_bitcast_fusion
  402.5 1.7 copy.370
  404.2 1.7 reshape.1317
  405.9 2.6 fusion.16
  408.6 3.7 all_gather.54
  413.0 1.5 fusion.7
  (210 shorter events, 35.1 us)
Async XLA Ops:
  6.5 49.7 %copy-start = (bf16[2048,512]{1,0:T(8,128)(2,1)S(1)}, bf16[2048,512]{1,0:T(8,128)(2,1)}, u32[]{:S(2)}) copy-start(bf16[2048,512]{1,0:T(8,128)(2,1)} %param.24) | copy-start | bytes 6291460
  6.5 49.7 %all-gather.6.cloned.1.call-start = ((), (), s32[]{:S(2)}) async-start(), calls=%async_computation.2 | async-start | bytes 1572864 | tf_op jit(solution)/shard_map/all_gather | solution.py:239
  11.2 5.6 %copy-start.29 = (f32[32]{0:T(128)S(1)}, f32[32]{0:T(128)}, u32[]{:S(2)}) copy-start(f32[32]{0:T(128)} %param.29) | copy-start | bytes 388
  11.2 5.6 %copy-start.24 = (f32[32,64]{1,0:T(8,128)S(1)}, f32[32,64]{1,0:T(8,128)}, u32[]{:S(2)}) copy-start(f32[32,64]{1,0:T(8,128)} %param.28) | copy-start | bytes 24580
  11.2 5.6 %copy-start.25 = (f32[32,64]{1,0:T(8,128)S(1)}, f32[32,64]{1,0:T(8,128)}, u32[]{:S(2)}) copy-start(f32[32,64]{1,0:T(8,128)} %param.27) | copy-start | bytes 24580
  11.2 31.2 %all-to-all-start = ((bf16[512,2,1024]{0,2,1:T(8,128)(2,1)}), bf16[512,2,1024]{0,2,1:T(8,128)(2,1)}, u32[]{:S(2)}, u32[]{:S(2)}) async-start(bf16[512,2,1024]{0,2,1:T(8,128)(2,1)} %bitcast.1078), calls=%async_computation | async-start | bytes 4194304 | tf_op jit(solution)/shard_map/all_to_all | solution.py:262
  32.9 3.9 copy-start.22
  32.9 4.2 copy-start.26
  32.9 4.9 %copy-start.27 = (f32[8]{0:T(128)S(1)}, f32[8]{0:T(128)}, u32[]{:S(2)}) copy-start(f32[8]{0:T(128)} %param.26) | copy-start | bytes 100
  37.1 44.4 %copy-start.14 = (f32[32,256]{1,0:T(8,128)}, f32[32,256]{1,0:T(8,128)S(1)}, u32[]{:S(2)}) copy-start(f32[32,256]{1,0:T(8,128)S(1)} %exp.69) | copy-start | bytes 98308
  42.4 9.0 %all-to-all-start.1 = ((bf16[512,2,1024]{0,2,1:T(8,128)(2,1)}), bf16[512,2,1024]{0,2,1:T(8,128)(2,1)}, u32[]{:S(2)}, u32[]{:S(2)}) async-start(bf16[512,2,1024]{0,2,1:T(8,128)(2,1)} %bitcast.1079), calls=%async_computation.1 | async-start | bytes 4194304 | tf_op jit(solution)/shard_map/all_to_all | solution.py:263
  56.3 3.9 copy-start.8
  58.9 2.8 copy-start.5
  60.2 1.5 copy-start.9
  106.1 7.1 %copy-start.12 = (f32[16,64,8]{1,2,0:T(8,128)}, f32[16,64,8]{1,2,0:T(8,128)S(1)}, u32[]{:S(2)}) copy-start(f32[16,64,8]{1,2,0:T(8,128)S(1)} %get-tuple-element.122) | copy-start | bytes 98308
  106.1 7.1 %copy-start.13 = (f32[16,64,8]{1,2,0:T(8,128)}, f32[16,64,8]{1,2,0:T(8,128)S(1)}, u32[]{:S(2)}) copy-start(f32[16,64,8]{1,2,0:T(8,128)S(1)} %get-tuple-element.123) | copy-start | bytes 98308
  107.1 2.0 copy-start.19
  107.1 2.0 copy-start.20
  167.2 159.3 %copy-start.11 = (f32[32,64,7]{1,2,0:T(8,128)S(1)}, f32[32,64,7]{1,2,0:T(8,128)}, u32[]{:S(2)}) copy-start(f32[32,64,7]{1,2,0:T(8,128)} %get-tuple-element.38) | copy-start | bytes 172036
  327.8 2.4 copy-start.2
  327.9 2.4 copy-start.15
  330.2 4.5 %copy-start.18 = (f32[32,16,64]{2,1,0:T(8,128)S(1)}, f32[32,16,64]{2,1,0:T(8,128)}, u32[]{:S(2)}) copy-start(f32[32,16,64]{2,1,0:T(8,128)} %param.32) | copy-start | bytes 393220
  334.7 1.0 copy-start.16
  334.7 0.9 copy-start.21
  337.1 3.6 copy-start.6
  337.2 3.6 copy-start.10
  338.5 5.0 %copy-start.28 = (bf16[2048,512]{1,0:T(8,128)(2,1)S(1)}, bf16[2048,512]{1,0:T(8,128)(2,1)}, u32[]{:S(2)}) copy-start(bf16[2048,512]{1,0:T(8,128)(2,1)} %param.20) | copy-start | bytes 6291460
  341.3 56.6 %collective-permute-start = (bf16[128,512]{0,1:T(8,128)(2,1)S(1)}, bf16[128,512]{0,1:T(8,128)(2,1)S(1)}, u32[]{:S(2)}, u32[]{:S(2)}) collective-permute-start(bf16[128,512]{0,1:T(8,128)(2,1)S(1)} %fusion.41), channel_id=1, source_target_pairs={{0,2},{2,4},{4,6},{6,8},{8,10},{10,12},{12,14},{14,16},{16,18},{18... | collective-permute-start | bytes 393224 | tf_op jit(solution)/shard_map/ppermute | solution.py:21
  398.0 1.2 copy-start.17
  398.7 2.0 copy-start.23
  405.9 6.3 %copy-start.3 = (bf16[2,512,1024]{2,1,0:T(8,128)(2,1)S(1)}, bf16[2,512,1024]{2,1,0:T(8,128)(2,1)}, u32[]{:S(2)}) copy-start(bf16[2,512,1024]{2,1,0:T(8,128)(2,1)} %copy.326) | copy-start | bytes 6291460
  408.5 4.5 %copy-start.4 = (bf16[2,512,1024]{2,1,0:T(8,128)(2,1)S(1)}, bf16[2,512,1024]{2,1,0:T(8,128)(2,1)}, u32[]{:S(2)}) copy-start(bf16[2,512,1024]{2,1,0:T(8,128)(2,1)} %copy.362) | copy-start | bytes 6291460
  408.6 4.5 %copy-start.7 = (bf16[256,1024]{1,0:T(8,128)(2,1)S(1)}, bf16[256,1024]{1,0:T(8,128)(2,1)}, u32[]{:S(2)}) copy-start(bf16[256,1024]{1,0:T(8,128)(2,1)} %all_gather.67) | copy-start | bytes 1572868
  413.0 1.6 copy-start.1
Sparse Core Ops, SparseCore 0:
  9.1 15.2 all-gather.5
where the time goes:
time: 426 us; the launch traced here: 421 us
  blocking collectives  209 us (49%)
  local copies, waits for them, and re-layouts  129 us (30%)
  other arithmetic  30.9 us (7%)
  matrix products  24.1 us (6%)
  between operations  14.6 us (3%)
  starting transfers between devices  12.8 us (3%)
    all_gather x12, blocking collectives, prefix_by_axis(): pieces = jax.tree.map(lambda part: lax.all_gather(part, axis), running)  155 us
    all_gather x1, blocking collectives, on_device(): lax.all_gather(state_mixed, 'tp', axis=1, tiled=True)  50.1 us
    unnamed x68, local copies, waits for them, and re-layouts  31 us
    pad x22, local copies, waits for them, and re-layouts, recur(): inclusive = lax.associative_scan(combine, segment_ends, axis=2)  27 us
    dot_general x6, matrix products, on_device(): jnp.dot(portion, weight, preferred_element_type=jnp.float32)  11.2 us
    add x1, other arithmetic, recur(): local_imag = cum_real * scaled[1] + cum_imag * scaled[0]  9.71 us
    squeeze x4, local copies, waits for them, and re-layouts, recur(): local_real = cum_real * scaled[0] - cum_imag * scaled[1]  9.3 us
  transfers between devices with their start and end apart: 4, of which 0 were waited for; matrix products, arithmetic and copies ran while one was open for 10% of the time, Pallas kernels for 0%

commit v1 on v0

v1 whole, which is shorter than its diff:
```python
import functools

import jax
import jax.numpy as jnp
from jax import lax
from jax.experimental import pallas as pl
from jax.experimental.pallas import tpu as pltpu
from jax.sharding import PartitionSpec as P

MESH = pl.DeviceIdType.MESH
F32 = jnp.float32
BF16 = jnp.bfloat16

TOK = 256
D = 2048
HALF = D // 2
WINDOW = 128
SEG = 16
CHUNKS = TOK // SEG
PAIRS = 16
LANES = PAIRS * 256
KV_HEADS = 4
SP_SIZES = {128: (8, 4, 4), 8: (2, 2, 2)}

HID, HALO, OUT = 0, 1, 2
N_OUT = 4


def dot(a, b):
    return jnp.dot(a, b, preferred_element_type=F32)


def dot_nt(a, b):
    return lax.dot_general(a, b, (((1,), (1,)), ((), ())), preferred_element_type=F32)


def cmul(a, b):
    return (a[0] * b[0] - a[1] * b[1], a[0] * b[1] + a[1] * b[0])


def csquares(a, times):
    for _ in range(times):
        a = cmul(a, a)
    return a


def log2(n):
    return n.bit_length() - 1


def kernel(
    sizes,
    hidden,
    w_query,
    w_key,
    w_value,
    w_hgate,
    w_sin,
    w_sgate,
    w_hout,
    w_sout,
    sink,
    base,
    drive_c,
    out_c,
    skip,
    shift,
    out,
    h_ref,
    win,
    wkv,
    wq,
    whg,
    wsg,
    who,
    wso,
    drive,
    cmat,
    tri,
    grow,
    shrink,
    decay,
    shift_tile,
    u_ref,
    us_ref,
    es_ref,
    x_ref,
    s_ref,
    tot_re,
    tot_im,
    ent_re,
    ent_im,
    q_ref,
    kv_ref,
    hg_ref,
    sg_ref,
    hm_ref,
    sm_ref,
    acc_ref,
    psend,
    precv,
    own_x,
    own_y,
    own_z,
    got_x,
    got_y,
    got_z,
    pre_z,
    w_sem,
    send_sem,
    recv_sem,
):
    nz, ny, nx = sizes
    n_sp = nz * ny * nx
    sp, tp = lax.axis_index("sp"), lax.axis_index("tp")
    z, y, x = sp // (ny * nx), (sp // nx) % ny, sp % nx
    other = 1 - tp
    nxt, prv = lax.rem(sp + 1, n_sp), lax.rem(sp + n_sp - 1, n_sp)

    loads = []

    def load(src, dst):
        copy = pltpu.make_async_copy(src, dst, w_sem.at[len(loads)])
        copy.start()
        loads.append(copy)
        return copy

    mine = pl.ds(pl.multiple_of(tp * HALF, HALF), HALF)
    theirs = pl.ds(pl.multiple_of(other * HALF, HALF), HALF)
    l_h = load(hidden, h_ref.at[:, mine])
    l_in = load(w_sin, win)
    l_k = load(w_key, wkv.at[:, 0:256])
    l_v = load(w_value, wkv.at[:, 256:512])
    l_q = load(w_query, wq)
    l_hg = load(w_hgate, whg)
    l_sg = load(w_sgate, wsg)
    l_ho = load(w_hout, who)
    l_so = load(w_sout, wso)

    def x_peer(r):
        return (sp - x + lax.rem(x + r, nx), tp)

    def y_peer(r):
        return (sp + (lax.rem(y + r, ny) - y) * nx, tp)

    def z_peer(r):
        return (sp + (lax.rem(z + r, nz) - z) * (nx * ny), tp)

    peers = [(sp, other), (nxt, tp), (prv, tp)]
    peers += [x_peer(r) for r in range(1, nx)]
    peers += [y_peer(r) for r in range(1, ny)]
    peers += [z_peer(r) for r in range(1, nz)]
    barrier = pltpu.get_barrier_semaphore()
    for peer in peers:
        pl.semaphore_signal(barrier, inc=1, device_id=peer, device_id_type=MESH)

    def remote(src, dst, number, device):
        return pltpu.make_async_remote_copy(
            src_ref=src,
            dst_ref=dst,
            send_sem=send_sem.at[number],
            recv_sem=recv_sem.at[number],
            device_id=device,
            device_id_type=MESH,
        )

    row = lax.broadcasted_iota(jnp.int32, (TOK, TOK), 0)
    col = lax.broadcasted_iota(jnp.int32, (TOK, TOK), 1)
    tri[0:TOK, :] = ((row // SEG == col // SEG) & (col <= row)).astype(F32).astype(BF16)
    srow = lax.broadcasted_iota(jnp.int32, (CHUNKS, TOK), 0)
    scol = lax.broadcasted_iota(jnp.int32, (CHUNKS, TOK), 1)
    tri[TOK:, :] = (scol // SEG == srow).astype(F32).astype(BF16)
    drive[...] = jnp.zeros_like(drive)
    cmat[...] = jnp.zeros_like(cmat)
    for i in range(PAIRS):
        rows, cols = slice((i % 4) * 32, (i % 4) * 32 + 32), slice(i * 256, i * 256 + 256)
        drive[rows, cols] = drive_c[i * 32 : i * 32 + 32, :]
        cmat[rows, cols] = out_c[i * 32 : i * 32 + 32, :]

    power = lax.broadcasted_iota(jnp.int32, (8, 128), 0) + 1
    ones, zeros = jnp.ones((8, 128), F32), jnp.zeros((8, 128), F32)
    for table, first in ((grow, 0), (shrink, 2)):
        for i in range(PAIRS):
            b = tuple(jnp.broadcast_to(base[first + k, i : i + 1, :], (8, 128)) for k in (0, 1))
            value = (ones, zeros)
            for bit in range(4):
                has = (power >> bit) & 1 == 1
                value = cmul(value, (jnp.where(has, b[0], ones), jnp.where(has, b[1], zeros)))
                if bit < 3:
                    b = cmul(b, b)
            cols = slice(i * 128, i * 128 + 128)
            upper = cmul(value, b)
            for k in (0, 1):
                table[k, 0:8, cols] = value[k]
                table[k, 8:16, cols] = upper[k]
    a_seg = csquares((base[0], base[1]), log2(SEG))
    a_dev = csquares(a_seg, log2(CHUNKS))
    a_line = csquares(a_dev, log2(nx))
    a_plane = csquares(a_line, log2(ny))

    rest = jnp.broadcast_to(shift[...][:, None, :], (2 * PAIRS, 16, TOK)).reshape(512, TOK)
    sums = None
    for k in range(3):
        part = rest.astype(BF16)
        term = dot_nt(tri[0:TOK, :], part)
        sums = term if sums is None else sums + term
        rest = rest - part.astype(F32)
    es_ref[...] = sums
    low = lax.broadcasted_iota(jnp.int32, (PAIRS, 128), 1) < 64
    lane = lax.broadcasted_iota(jnp.int32, (PAIRS, 128), 1)
    total_shift = jnp.zeros((PAIRS, 128), F32)
    for c in range(CHUNKS):
        if c % 8 == 0:
            shift_tile[...] = shift[:, c * SEG : c * SEG + 128]
            even = shift_tile[pl.ds(0, PAIRS, stride=2), :]
            odd = shift_tile[pl.ds(1, PAIRS, stride=2), :]
        inside = lane // SEG == c % 8
        s = jnp.where(
            low,
            jnp.sum(jnp.where(inside, even, 0.0), axis=1, keepdims=True),
            jnp.sum(jnp.where(inside, odd, 0.0), axis=1, keepdims=True),
        )
        total_shift = total_shift + s
        decay[c] = jnp.exp(s)

    pl.semaphore_wait(barrier, len(peers))
    send_h = remote(hidden, h_ref.at[:, mine], HID, (sp, other))
    send_h.start()

    l_h.wait()
    l_in.wait()
    u_ref[...] = dot(h_ref[:, mine], win[mine, :])
    send_h.wait_recv()
    u = (u_ref[...] + dot(h_ref[:, theirs], win[theirs, :])).astype(BF16).astype(F32)
    u_ref[...] = u
    us_ref[...] = (u * jnp.exp(-es_ref[...])).astype(BF16)

    for i in range(PAIRS):
        cols, narrow = slice(i * 256, i * 256 + 256), slice(i * 128, i * 128 + 128)
        j = i // 4
        push = dot(us_ref[:, j * 128 : j * 128 + 128], drive[:, cols])
        push = (push[:, :128].reshape(CHUNKS, SEG, 128), push[:, 128:].reshape(CHUNKS, SEG, 128))
        back = (shrink[0, :, narrow][None], shrink[1, :, narrow][None])
        w = cmul(push, back)
        w = jnp.concatenate([part.reshape(TOK, 128).astype(BF16) for part in w], axis=1)
        summed = dot(tri[...], w)
        x_ref[:, cols] = summed[:TOK]
        tot_re[i * 16 : i * 16 + 16, :] = summed[TOK:, :128]
        tot_im[i * 16 : i * 16 + 16, :] = summed[TOK:, 128:]

    def chunk_scan(state, keep):
        for c in range(CHUNKS):
            at = pl.ds(c, PAIRS, stride=CHUNKS)
            if keep:
                ent_re[at, :] = state[0]
                ent_im[at, :] = state[1]
            e = decay[c]
            state = cmul(
                (state[0] + tot_re[at, :], state[1] + tot_im[at, :]), (a_seg[0] * e, a_seg[1] * e)
            )
        return state

    flat_zero = jnp.zeros((PAIRS, 128), F32)
    flat_one = jnp.ones((PAIRS, 128), F32)
    local = chunk_scan((flat_zero, flat_zero), False)
    own_x[0], own_x[1], own_x[2] = local[0], local[1], total_shift
    number = OUT + N_OUT
    sends_x = []
    for r in range(1, nx):
        copy = remote(own_x, got_x.at[r - 1], number, x_peer(r))
        copy.start()
        sends_x.append(copy)
        number += 1

    l_k.wait()
    l_v.wait()
    kv_ref[WINDOW:, :] = dot(h_ref[...], wkv[...]).astype(BF16)
    halo = remote(kv_ref.at[TOK : TOK + WINDOW, :], kv_ref.at[0:WINDOW, :], HALO, (nxt, tp))
    l_q.wait()
    q_ref[...] = (dot(h_ref[...], wq[...]).astype(BF16).astype(F32) * 0.125)
    halo.start()

    def stage(got, own, a, at, count):
        factors = []
        for r in range(1, count):
            e = jnp.exp(got[r - 1, 2])
            factors.append((a[0] * e, a[1] * e))
        before, through = (flat_zero, flat_zero), (flat_one, flat_zero)
        total_s = own[2]
        for r in range(count - 1, 0, -1):
            earlier = r <= at
            f = factors[r - 1]
            new = cmul(f, before)
            before = (
                jnp.where(earlier, new[0] + got[r - 1, 0], before[0]),
                jnp.where(earlier, new[1] + got[r - 1, 1], before[1]),
            )
            new = cmul(f, through)
            through = (
                jnp.where(earlier, new[0], through[0]),
                jnp.where(earlier, new[1], through[1]),
            )
            total_s = total_s + got[r - 1, 2]
        e = jnp.exp(own[2])
        new = cmul((a[0] * e, a[1] * e), before)
        total = (new[0] + own[0], new[1] + own[1])
        for r in range(count - 1, 0, -1):
            later = r > at
            new = cmul(factors[r - 1], total)
            total = (
                jnp.where(later, new[0] + got[r - 1, 0], total[0]),
                jnp.where(later, new[1] + got[r - 1, 1], total[1]),
            )
        return before, through, total, total_s

    for copy in sends_x:
        copy.wait_recv()
    before_x, through_x, total, total_s = stage(got_x, own_x, a_dev, x, nx)
    own_y[0], own_y[1], own_y[2] = total[0], total[1], total_s
    sends_y = []
    for r in range(1, ny):
        copy = remote(own_y, got_y.at[r - 1], number, y_peer(r))
        copy.start()
        sends_y.append(copy)
        number += 1

    l_hg.wait()
    hg_ref[...] = dot(h_ref[...], whg[...]).astype(BF16).astype(F32)
    l_sg.wait()
    sg_ref[...] = dot(h_ref[...], wsg[...]).astype(BF16).astype(F32)

    for copy in sends_y:
        copy.wait_recv()
    before_y, through_y, total, total_s = stage(got_y, own_y, a_line, y, ny)
    own_z[0], own_z[1], own_z[2] = total[0], total[1], total_s
    sends_z = []
    for r in range(1, nz):
        copy = remote(own_z, got_z.at[r - 1], number, z_peer(r))
        pl.when(z + r < nz)(copy.start)
        sends_z.append(copy)
        number += 1

    halo.wait_recv()
    qi = lax.rem(lax.broadcasted_iota(jnp.int32, (2 * WINDOW, 2 * WINDOW), 0), WINDOW)
    key_at = lax.broadcasted_iota(jnp.int32, (2 * WINDOW, 2 * WINDOW), 1)
    inside = (key_at > qi) & (key_at <= qi + WINDOW)
    left = lax.broadcasted_iota(jnp.int32, (WINDOW, 128), 1) < 64
    for n in range(TOK // WINDOW):
        allowed = inside & ((key_at >= WINDOW) | (sp > 0)) if n == 0 else inside
        rows = slice(n * WINDOW, (n + 1) * WINDOW)
        keys = slice(n * WINDOW, (n + 2) * WINDOW)
        for h in range(KV_HEADS):
            q = q_ref[rows, h * 128 : h * 128 + 128]
            turned = pltpu.roll(q, 64, 1)
            in_half = left if h % 2 == 0 else jnp.logical_not(left)
            first, second = (q, turned) if h % 2 == 0 else (turned, q)
            stacked = jnp.concatenate(
                [jnp.where(in_half, part, 0.0).astype(BF16) for part in (first, second)], axis=0
            )
            tile = slice((h // 2) * 128, (h // 2) * 128 + 128)
            scores = dot_nt(stacked, kv_ref[keys, tile])
            scores = jnp.where(allowed, scores, -1e30)
            first_row = lax.broadcasted_iota(jnp.int32, (2 * WINDOW, 1), 0) < WINDOW
            sink_col = jnp.where(first_row, sink[2 * h], sink[2 * h + 1])
            peak = jnp.maximum(jnp.max(scores, axis=1, keepdims=True), sink_col)
            e = jnp.exp(scores - peak)
            total = jnp.sum(e, axis=1, keepdims=True) + jnp.exp(sink_col - peak)
            vtile = slice(256 + (h // 2) * 128, 256 + (h // 2) * 128 + 128)
            mixed = dot(e.astype(BF16), kv_ref[keys, vtile]) / total
            a, b = mixed[:WINDOW], mixed[WINDOW:]
            if h % 2 == 0:
                joined = jnp.where(left, a, pltpu.roll(b, 64, 1))
            else:
                joined = jnp.where(left, pltpu.roll(a, 64, 1), b)
            gate = jax.nn.sigmoid(hg_ref[rows, h * 128 : h * 128 + 128])
            hm_ref[rows, h * 128 : h * 128 + 128] = (gate * joined).astype(BF16)
    l_ho.wait()
    acc_ref[...] = dot(hm_ref[...], who[...])

    pre_z[...] = jnp.zeros_like(pre_z)
    for r in range(nz - 1, 0, -1):

        @pl.when(r <= z)
        def _(r=r):
            sends_z[r - 1].wait_recv()
            e = jnp.exp(got_z[r - 1, 2])
            new = cmul((a_plane[0] * e, a_plane[1] * e), (pre_z[0], pre_z[1]))
            pre_z[0] = new[0] + got_z[r - 1, 0]
            pre_z[1] = new[1] + got_z[r - 1, 1]

    carry = cmul(through_y, (pre_z[0], pre_z[1]))
    carry = cmul(through_x, (before_y[0] + carry[0], before_y[1] + carry[1]))
    chunk_scan((before_x[0] + carry[0], before_x[1] + carry[1]), True)

    for j in range(4):
        for k in range(4):
            i = 4 * j + k
            narrow = slice(i * 128, i * 128 + 128)
            state = tuple(
                x_ref[:, i * 256 + 128 * part : i * 256 + 128 * part + 128].reshape(CHUNKS, SEG, 128)
                + entry[i * 16 : i * 16 + 16, :][:, None, :]
                for part, entry in ((0, ent_re), (1, ent_im))
            )
            state = cmul(state, (grow[0, :, narrow][None], grow[1, :, narrow][None]))
            s_ref[:, k * 256 : k * 256 + 128] = state[0].reshape(TOK, 128).astype(BF16)
            s_ref[:, k * 256 + 128 : k * 256 + 256] = state[1].reshape(TOK, 128).astype(BF16)
        cols = slice(j * 128, j * 128 + 128)
        rec = dot_nt(s_ref[...], cmat[:, j * 1024 : j * 1024 + 1024])
        rec = rec * jnp.exp(es_ref[:, cols]) + skip[:, cols] * u_ref[:, cols]
        gate = jax.nn.sigmoid(sg_ref[:, cols])
        sm_ref[:, cols] = (gate * jax.nn.gelu(rec)).astype(BF16)

    l_so.wait()
    outs = []
    for k in range(N_OUT):
        cols = pl.ds(pl.multiple_of(other * HALF + k * 256, 256), 256)
        psend[k] = (acc_ref[:, cols] + dot(sm_ref[...], wso[:, cols])).astype(BF16)
        copy = remote(psend.at[k], precv.at[k], OUT + k, (sp, other))
        copy.start()
        outs.append(copy)
    for k in range(N_OUT):
        cols = pl.ds(pl.multiple_of(tp * HALF + k * 256, 256), 256)
        own = acc_ref[:, cols] + dot(sm_ref[...], wso[:, cols])
        outs[k].wait_recv()
        out[:, k * 256 : k * 256 + 256] = (own + precv[k].astype(F32)).astype(BF16)

    send_h.wait_send()
    halo.wait_send()
    for copy in sends_x + sends_y + outs:
        copy.wait_send()
    for r in range(1, nz):
        pl.when(z + r < nz)(sends_z[r - 1].wait_send)


def placed(re, im):
    groups, rows, states = re.shape
    re = re.reshape(groups // 2, 2, rows, states)
    im = im.reshape(groups // 2, 2, rows, states)
    none = jnp.zeros_like(re[:, 0])
    even = jnp.concatenate([re[:, 0], none, im[:, 0], none], axis=-1)
    odd = jnp.concatenate([none, re[:, 1], none, im[:, 1]], axis=-1)
    return jnp.stack([even, odd], axis=1).reshape(groups * rows, 4 * states).astype(BF16)


def on_device(
    sizes,
    hidden,
    query_weight,
    key_weight,
    value_weight,
    head_gate_weight,
    state_in_weight,
    state_gate_weight,
    sink_logit,
    decay_real,
    decay_frequency,
    log_step,
    input_real,
    input_imaginary,
    output_real,
    output_imaginary,
    skip_weight,
    decay_shift,
    head_out_weight,
    state_out_weight,
):
    nz, ny, nx = sizes
    stepsize = jnp.exp(log_step)[:, None]
    log_magnitude = decay_real * stepsize
    rotation = decay_frequency * stepsize
    magnitude, inverse = jnp.exp(log_magnitude), jnp.exp(-log_magnitude)
    cosine, sine = jnp.cos(rotation), jnp.sin(rotation)
    base_real, base_imag = magnitude * cosine, magnitude * sine
    denominator = decay_real * decay_real + decay_frequency * decay_frequency
    less_real = base_real - 1.0
    zoh_real = ((less_real * decay_real + base_imag * decay_frequency) / denominator)[:, None, :]
    zoh_imag = ((base_imag * decay_real - less_real * decay_frequency) / denominator)[:, None, :]
    in_real, in_imag = input_real.transpose(0, 2, 1), input_imaginary.transpose(0, 2, 1)
    drive = placed(
        zoh_real * in_real - zoh_imag * in_imag, zoh_real * in_imag + zoh_imag * in_real
    )
    outm = placed(output_real, -output_imaginary)
    base = jnp.stack([base_real, base_imag, inverse * cosine, -inverse * sine]).reshape(
        4, PAIRS, 128
    )
    skip = skip_weight.reshape(1, 512)

    vmem = pl.BlockSpec(memory_space=pltpu.VMEM)
    hbm = pl.BlockSpec(memory_space=pl.ANY)
    n_remote = OUT + N_OUT + (nx - 1) + (ny - 1) + (nz - 1)
    scratch = [
        ((TOK, D), BF16),
        ((D, 512), BF16),
        ((D, 512), BF16),
        ((D, 512), BF16),
        ((D, 512), BF16),
        ((D, 512), BF16),
        ((512, D), BF16),
        ((512, D), BF16),
        ((128, LANES), BF16),
        ((128, LANES), BF16),
        ((TOK + CHUNKS, TOK), BF16),
        ((2, SEG, PAIRS * 128), F32),
        ((2, SEG, PAIRS * 128), F32),
        ((CHUNKS, PAIRS, 128), F32),
        ((2 * PAIRS, 128), F32),
        ((TOK, 512), F32),
        ((TOK, 512), BF16),
        ((TOK, 512), F32),
        ((TOK, LANES), F32),
        ((TOK, 1024), BF16),
        ((PAIRS * CHUNKS, 128), F32),
        ((PAIRS * CHUNKS, 128), F32),
        ((PAIRS * CHUNKS, 128), F32),
        ((PAIRS * CHUNKS, 128), F32),
        ((TOK, 512), F32),
        ((TOK + WINDOW, 512), BF16),
        ((TOK, 512), F32),
        ((TOK, 512), F32),
        ((TOK, 512), BF16),
        ((TOK, 512), BF16),
        ((TOK, D), F32),
        ((N_OUT, TOK, 256), BF16),
        ((N_OUT, TOK, 256), BF16),
        ((3, PAIRS, 128), F32),
        ((3, PAIRS, 128), F32),
        ((3, PAIRS, 128), F32),
        ((nx - 1, 3, PAIRS, 128), F32),
        ((ny - 1, 3, PAIRS, 128), F32),
        ((nz - 1, 3, PAIRS, 128), F32),
        ((2, PAIRS, 128), F32),
    ]
    return pl.pallas_call(
        functools.partial(kernel, sizes),
        out_shape=jax.ShapeDtypeStruct((TOK, HALF), BF16),
        in_specs=[hbm] * 9 + [pl.BlockSpec(memory_space=pltpu.SMEM)] + [vmem] * 5,
        out_specs=vmem,
        scratch_shapes=[pltpu.VMEM(shape, dtype) for shape, dtype in scratch]
        + [
            pltpu.SemaphoreType.DMA((9,)),
            pltpu.SemaphoreType.DMA((n_remote,)),
            pltpu.SemaphoreType.DMA((n_remote,)),
        ],
        compiler_params=pltpu.CompilerParams(
            collective_id=0, has_side_effects=True, vmem_limit_bytes=60 * 1024 * 1024
        ),
        name="layer",
    )(
        hidden,
        query_weight,
        key_weight,
        value_weight,
        head_gate_weight,
        state_in_weight,
        state_gate_weight,
        head_out_weight,
        state_out_weight,
        sink_logit,
        base,
        drive,
        outm,
        skip,
        decay_shift,
    )


def solution(mesh):
    sizes = SP_SIZES[mesh.shape["sp"]]
    in_specs = (
        P("sp", "tp"),
        P(None, "tp"),
        P(None, "tp"),
        P(None, "tp"),
        P(None, "tp"),
        P(None, "tp"),
        P(None, "tp"),
        P("tp"),
        P("tp", None),
        P("tp", None),
        P("tp"),
        P("tp", None, None),
        P("tp", None, None),
        P("tp", None, None),
        P("tp", None, None),
        P("tp", None),
        P("tp", "sp"),
        P("tp", None),
        P("tp", None),
    )
    return jax.shard_map(
        functools.partial(on_device, sizes),
        mesh=mesh,
        in_specs=in_specs,
        out_specs=P("sp", "tp"),
        check_vma=False,
    )
```

time: 426 us -> 44.1 us (0.10)
  the two profiles are of different devices: /device:TPU:225 before, /device:TPU:193 now
where the time goes in v1:
time: 44.1 us; the launch traced here: 43.8 us
  Pallas kernels  33.8 us (77%)
  other arithmetic  5.59 us (13%)
  local copies, waits for them, and re-layouts  4.34 us (10%)
    pallas_call x1, Pallas kernels, on_device(): pl.pallas_call(functools.partial(kernel, sizes), out_shape=jax.ShapeDtype...  33.8 us
    another operation x3, other arithmetic  3.05 us
    unnamed x4, local copies, waits for them, and re-layouts  1.95 us
    another operation x3, other arithmetic, placed(): jnp.stack([even, odd], axis=1).reshape(groups * rows, 4 * states)  1.03 us
    div x1, other arithmetic, on_device(): (less_real * decay_real + base_imag * decay_frequency) / denominator  0.9 us

profile of v1, /device:TPU:193, one launch (start us, length us, event | category | flops | bytes accessed | tf_op | source)
XLA Modules:
  0.0 43.8 jit_solution(15126815537899914537)
XLA Ops:
  0.0 0.7 %exp.9 = f32[32]{0:T(128)S(1)} exponential(f32[32]{0:T(128)} %param.29) | non-fusion elementwise | bytes 256 | tf_op jit(solution)/shard_map/exp | solution.py:468
  0.7 0.9 %fusion.8 = (f32[32,64]{1,0:T(8,128)S(1)}, f32[32,64]{1,0:T(8,128)S(1)}, f32[32,64]{1,0:T(8,128)S(1)}, f32[32,64]{1,0:T(8,128)S(1)}, f32[32,64]{1,0:T(8,128)S(1)}, /*index=5*/f32[32,64]{1,0:T(8,128)S(1)}) fusion(f32[32,64]{1,0:T(8,128)} %param.28, f32[32,64]{1,0:T(8,128)} %param.27, f32[32]{0:T(128)S(1)} %exp.9), kind=kLoop, calls=%fused_computation.32 | loop fusion | flops 40960 | bytes 65664 | tf_op jit(solution)/shard_map/div | solution.py:476
  1.6 0.1 stack.42
  1.6 0.1 stack.41
  1.7 0.1 stack.40
  1.8 0.1 stack.39
  1.8 0.6 %pad_maximum_fusion.10.base = f32[4,16,128]{2,1,0:T(8,128)} fusion(f32[1,16,128]{2,1,0:T(8,128)S(1)} %stack.42, f32[1,16,128]{2,1,0:T(8,128)S(1)} %stack.41, f32[1,16,128]{2,1,0:T(8,128)S(1)} %stack.40, f32[1,16,128]{2,1,0:T(8,128)S(1)} %stack.39), kind=kLoop, calls=%fused_computation.29 | loop fusion | flops 24576 | bytes 65536 | tf_op jit(solution)/shard_map/stack | solution.py:483
  2.5 1.0 %negate_convert_fusion = bf16[32,16,64]{2,1,0:T(8,128)(2,1)S(1)} fusion(f32[32,16,64]{2,1,0:T(8,128)} %param.33), kind=kLoop, calls=%fused_computation.2 | loop fusion | flops 65536 | bytes 196608 | tf_op jit(solution)/shard_map/convert.17
  3.4 1.0 %convert.62 = bf16[32,16,64]{2,1,0:T(8,128)(2,1)S(1)} convert(f32[32,16,64]{2,1,0:T(8,128)} %param.32) | non-fusion elementwise | flops 32768 | bytes 196608 | tf_op jit(solution)/shard_map/convert.19
  4.4 0.0 copy-start
  4.4 1.1 %subtract_convert_fusion = (bf16[32,64,16]{1,2,0:T(8,128)(2,1)S(1)}, bf16[32,64,16]{1,2,0:T(8,128)(2,1)S(1)}) fusion(f32[32,64,16]{1,2,0:T(8,128)} %param.31, f32[32,64,16]{1,2,0:T(8,128)} %param.30, f32[32,64]{1,0:T(8,128)S(1)} %get-tuple-element.24, f32[32,64]{1,0:T(8,128)S(1)} %get-tuple-element.19), kind=kLoop, calls=%fused_computation.4 | loop fusion | flops 262144 | bytes 409600 | tf_op jit(solution)/shard_map/convert.39
  5.6 0.3 fusion.7
  5.9 0.7 %copy.35 = bf16[16,2,16,256]{3,2,1,0:T(8,128)(2,1)} copy(bf16[16,2,16,256]{3,2,0,1:T(8,128)(2,1)S(1)} %pad_maximum_fusion) | data formatting | bytes 524288 | tf_op jit(solution)/shard_map/stack | solution.py:442
  6.7 0.7 %pad_maximum_fusion.1 = bf16[16,2,16,256]{3,2,1,0:T(8,128)(2,1)} fusion(bf16[16,1,16,256]{3,2,1,0:T(8,128)(2,1)S(1)} %get-tuple-element.16, bf16[16,1,16,256]{3,2,1,0:T(8,128)(2,1)S(1)} %get-tuple-element.15), kind=kLoop, calls=%fused_computation.1 | loop fusion | flops 131072 | bytes 524288 | tf_op jit(solution)/shard_map/stack | solution.py:442
  7.4 0.0 copy-done
  7.4 0.1 copy.41
  7.5 0.7 %reshape.35.skip = f32[1,512]{1,0:T(1,128)} reshape(f32[32,16]{1,0:T(8,128)S(1)} %copy.41) | data formatting | bytes 4096 | tf_op jit(solution)/shard_map/reshape | solution.py:486
  8.1 33.8 %layer.1 = bf16[256,1024]{1,0:T(8,128)(2,1)} custom-call(bf16[256,1024]{1,0:T(8,128)(2,1)} %hidden.1, bf16[2048,512]{1,0:T(8,128)(2,1)} %w_query.1, bf16[2048,256]{1,0:T(8,128)(2,1)} %w_key.1, bf16[2048,256]{1,0:T(8,128)(2,1)} %w_value.1, bf16[2048,512]{1,0:T(8,128)(2,1)} %w_hgate.1, bf16[2048,512]{1,0:T(8,128)(2,1)} %w_sin.1, bf16[2048,512]{1,0:T(8,128)(2,1)} %w_sgate.1, ...), custom_call_target="tpu_custom_call" | custom-call | tf_op jit(solution)/shard_map/layer/pallas_call | solution.py:533
  42.0 1.9 %copy.51 = bf16[256,1024]{1,0:T(8,128)(2,1)} copy(bf16[256,1024]{1,0:T(8,128)(2,1)} %layer.1) | data formatting | bytes 1048576
  (4 shorter events, 0.1 us)
Async XLA Ops:
  4.4 2.9 %copy-start = (f32[32,16]{0,1:T(8,128)S(1)}, f32[32,16]{0,1:T(8,128)}, u32[]{:S(2)}) copy-start(f32[32,16]{0,1:T(8,128)} %param.34) | copy-start | bytes 6148

commit v2 on v1

v2 whole, which is shorter than its diff:
```python
import functools

import jax
import jax.numpy as jnp
from jax import lax
from jax.experimental import pallas as pl
from jax.experimental.pallas import tpu as pltpu
from jax.sharding import PartitionSpec as P

MESH = pl.DeviceIdType.MESH
F32 = jnp.float32
BF16 = jnp.bfloat16

TOK = 256
D = 2048
HALF = D // 2
WINDOW = 128
SEG = 16
CHUNKS = TOK // SEG
PAIRS = 16
LANES = PAIRS * 256
KV_HEADS = 4
SP_SIZES = {128: (8, 4, 4), 8: (2, 2, 2)}

N_OUT = 4


def dot(a, b):
    return jnp.dot(a, b, preferred_element_type=F32)


def dot_nt(a, b):
    return lax.dot_general(a, b, (((1,), (1,)), ((), ())), preferred_element_type=F32)


def cmul(a, b):
    return (a[0] * b[0] - a[1] * b[1], a[0] * b[1] + a[1] * b[0])


def csquares(a, times):
    for _ in range(times):
        a = cmul(a, a)
    return a


def log2(n):
    return n.bit_length() - 1


def kernel(sizes, *refs):
    nz, ny, nx = sizes
    plane = ny * nx
    (
        hidden,
        w_query,
        w_key,
        w_value,
        w_hgate,
        w_sin,
        w_sgate,
        w_hout,
        w_sout,
        sink_in,
        step_in,
        real_in,
        freq_in,
        in_re_in,
        in_im_in,
        out_re_in,
        out_im_in,
        skip_in,
        shift_in,
        out,
        sink,
        log_step,
        decay_real,
        decay_freq,
        in_re,
        in_im,
        out_re,
        out_im,
        skip_t,
        shift,
        h_ref,
        win,
        wkv,
        wq,
        whg,
        wsg,
        who,
        wso,
        drive,
        cmat,
        mmat,
        c_ref,
        tri,
        grow,
        shrink,
        decay,
        pair_tile,
        u_ref,
        us_ref,
        es_ref,
        ed_ref,
        w_ref,
        s_ref,
        g_ref,
        yl_ref,
        tot_re,
        tot_im,
        ent_re,
        ent_im,
        pow_re,
        pow_im,
        q_ref,
        kv_ref,
        hg_ref,
        sg_ref,
        hm_ref,
        sm_ref,
        acc_ref,
        psend,
        precv,
        s_buf,
        l_buf,
        zs_buf,
        zl_buf,
        pre,
        load_sem,
        h_sem,
        halo_sem,
        out_send,
        out_recv,
        s_send,
        s_recv,
        l_send,
        l_recv,
        zs_send,
        zs_recv,
        zl_send,
        zl_recv,
        ready_plane,
        ready_z,
        ready_halo,
    ) = refs
    sp, tp = lax.axis_index("sp"), lax.axis_index("tp")
    z, m = sp // plane, sp % plane
    other = 1 - tp

    loads = []

    def load(src, dst):
        copy = pltpu.make_async_copy(src, dst, load_sem.at[len(loads)])
        copy.start()
        loads.append(copy)
        return copy

    def remote(src, dst, send, recv, device):
        return pltpu.make_async_remote_copy(
            src_ref=src,
            dst_ref=dst,
            send_sem=send,
            recv_sem=recv,
            device_id=device,
            device_id_type=MESH,
        )

    mine = pl.ds(pl.multiple_of(tp * HALF, HALF), HALF)
    theirs = pl.ds(pl.multiple_of(other * HALF, HALF), HALF)
    l_h = load(hidden, h_ref.at[:, mine])
    small = [
        load(src, dst)
        for src, dst in (
            (step_in, log_step),
            (real_in, decay_real),
            (freq_in, decay_freq),
            (shift_in, shift),
            (in_re_in, in_re),
            (in_im_in, in_im),
            (out_re_in, out_re),
            (out_im_in, out_im),
            (skip_in, skip_t),
            (sink_in, sink),
        )
    ]
    l_in = load(w_sin, win)

    barrier = pltpu.get_barrier_semaphore()

    def signal(semaphore, device):
        pl.semaphore_signal(semaphore, inc=1, device_id=device, device_id_type=MESH)

    def when(condition, act, *args):
        pl.when(condition)(functools.partial(act, *args))

    crosses = jnp.logical_and(m == plane - 1, z < nz - 1)
    crossed = jnp.logical_and(m == 0, z > 0)
    signal(barrier, (sp, other))
    for r in range(1, plane):
        when(m + r < plane, signal, barrier, (sp + r, tp))
    for r in range(1, nz):
        when(z + r < nz, signal, barrier, (sp + r * plane, tp))
    when(crosses, signal, barrier, (sp + 1, tp))
    pl.semaphore_wait(barrier, 1 + m + z + crossed.astype(jnp.int32))
    l_h.wait()
    send_h = remote(h_ref.at[:, mine], h_ref.at[:, mine], h_sem.at[0], h_sem.at[1], (sp, other))
    send_h.start()
    for r in range(1, plane):
        when(m >= r, signal, ready_plane, (sp - r, tp))
    for r in range(1, nz):
        when(z >= r, signal, ready_z, (sp - r * plane, tp))
    when(crossed, signal, ready_halo, (sp - 1, tp))
    l_k = load(w_key, wkv.at[:, 0:256])
    l_v = load(w_value, wkv.at[:, 256:512])
    l_q = load(w_query, wq)

    for copy in small:
        copy.wait()
    low = lax.broadcasted_iota(jnp.int32, (PAIRS, 128), 1) < 64

    def paired(value):
        pair_tile[...] = jnp.concatenate([value, value], axis=1)
        even = pair_tile[pl.ds(0, PAIRS, stride=2), :]
        odd = pair_tile[pl.ds(1, PAIRS, stride=2), :]
        return jnp.where(low, even, odd)

    pair_row = lax.broadcasted_iota(jnp.int32, (PAIRS, 128), 0)
    step = jnp.zeros((PAIRS, 128), F32)
    for i in range(PAIRS):
        step = jnp.where(
            pair_row == i, jnp.where(low, log_step[2 * i], log_step[2 * i + 1]), step
        )
    step = jnp.exp(step)
    real, freq = paired(decay_real[...]), paired(decay_freq[...])
    magnitude, inverse = jnp.exp(real * step), jnp.exp(-(real * step))
    cosine, sine = jnp.cos(freq * step), jnp.sin(freq * step)
    base = (magnitude * cosine, magnitude * sine)
    base_inv = (inverse * cosine, -(inverse * sine))
    denominator = real * real + freq * freq
    less = base[0] - 1.0
    zoh = (
        (less * real + base[1] * freq) / denominator,
        (base[1] * real - less * freq) / denominator,
    )

    row = lax.broadcasted_iota(jnp.int32, (TOK, TOK), 0)
    col = lax.broadcasted_iota(jnp.int32, (TOK, TOK), 1)
    tri[0:TOK, :] = ((row // SEG == col // SEG) & (col <= row)).astype(F32).astype(BF16)
    srow = lax.broadcasted_iota(jnp.int32, (CHUNKS, TOK), 0)
    scol = lax.broadcasted_iota(jnp.int32, (CHUNKS, TOK), 1)
    tri[TOK:, :] = (scol // SEG == srow).astype(F32).astype(BF16)
    drive[...] = jnp.zeros_like(drive)
    for i in range(PAIRS):
        factor = (zoh[0][i : i + 1, :], zoh[1][i : i + 1, :])
        first = (i % 4) * 32
        value = cmul(factor, tuple(jnp.concatenate([t[2 * i], t[2 * i + 1]], axis=1) for t in (in_re, in_im)))
        for part in (0, 1):
            cols = slice(i * 256 + part * 128, i * 256 + part * 128 + 128)
            drive[first : first + 16, cols] = jnp.where(low, value[part], 0.0).astype(BF16)
            drive[first + 16 : first + 32, cols] = jnp.where(low, 0.0, value[part]).astype(BF16)

    power = lax.broadcasted_iota(jnp.int32, (8, 128), 0) + 1
    ones, zeros = jnp.ones((8, 128), F32), jnp.zeros((8, 128), F32)
    for table, root in ((grow, base), (shrink, base_inv)):
        for i in range(PAIRS):
            b = tuple(jnp.broadcast_to(part[i : i + 1, :], (8, 128)) for part in root)
            value = (ones, zeros)
            for bit in range(4):
                has = (power >> bit) & 1 == 1
                value = cmul(value, (jnp.where(has, b[0], ones), jnp.where(has, b[1], zeros)))
                if bit < 3:
                    b = cmul(b, b)
            cols = slice(i * 128, i * 128 + 128)
            upper = cmul(value, b)
            for k in (0, 1):
                table[k, 0:8, cols] = value[k]
                table[k, 8:16, cols] = upper[k]
    a_seg = csquares(base, log2(SEG))
    a_dev = csquares(a_seg, log2(CHUNKS))
    a_plane = csquares(a_dev, log2(plane))

    def shift_sums(mask):
        rest = jnp.broadcast_to(shift[...][:, None, :], (2 * PAIRS, 16, TOK)).reshape(512, TOK)
        sums = None
        for _ in range(3):
            part = rest.astype(BF16)
            term = dot_nt(mask, part)
            sums = term if sums is None else sums + term
            rest = rest - part.astype(F32)
        return sums

    es_ref[...] = shift_sums(tri[0:TOK, :])
    lane = lax.broadcasted_iota(jnp.int32, (PAIRS, 128), 1)
    total_shift = jnp.zeros((PAIRS, 128), F32)
    for c in range(CHUNKS):
        if c % 8 == 0:
            pair_tile[...] = shift[:, c * SEG : c * SEG + 128]
            even = pair_tile[pl.ds(0, PAIRS, stride=2), :]
            odd = pair_tile[pl.ds(1, PAIRS, stride=2), :]
        inside = lane // SEG == c % 8
        s = jnp.where(
            low,
            jnp.sum(jnp.where(inside, even, 0.0), axis=1, keepdims=True),
            jnp.sum(jnp.where(inside, odd, 0.0), axis=1, keepdims=True),
        )
        total_shift = total_shift + s
        decay[c] = jnp.exp(s)
    s_buf[m] = total_shift

    l_in.wait()
    u_ref[...] = dot(h_ref[:, mine], win[mine, :])
    send_h.wait_recv()
    l_hg = load(w_hgate, whg)
    l_sg = load(w_sgate, wsg)
    l_ho = load(w_hout, who)
    l_so = load(w_sout, wso)
    u = (u_ref[...] + dot(h_ref[:, theirs], win[theirs, :])).astype(BF16).astype(F32)
    u_ref[...] = u
    us_ref[...] = (u * jnp.exp(-es_ref[...])).astype(BF16)

    when(m < plane - 1, pl.semaphore_wait, ready_plane, plane - 1 - m)

    def plane_copy(buf, send, recv, k):
        return remote(buf.at[m], buf.at[m], send.at[k], recv.at[m], (z * plane + k, tp))

    def plane_wait(buf, send, recv, k):
        remote(buf.at[k], buf.at[k], send.at[k], recv.at[k], (z * plane + k, tp)).wait_recv()

    for k in range(plane):
        when(m != k, plane_copy(s_buf, s_send, s_recv, k).start)

    for i in range(PAIRS):
        cols, narrow = slice(i * 256, i * 256 + 256), slice(i * 128, i * 128 + 128)
        j = i // 4
        push = dot(us_ref[:, j * 128 : j * 128 + 128], drive[:, cols])
        push = (push[:, :128].reshape(CHUNKS, SEG, 128), push[:, 128:].reshape(CHUNKS, SEG, 128))
        back = (shrink[0, :, narrow][None], shrink[1, :, narrow][None])
        w = cmul(push, back)
        w = jnp.concatenate([part.reshape(TOK, 128).astype(BF16) for part in w], axis=1)
        w_ref[:, cols] = w
        summed = dot(tri[TOK:, :], w)
        tot_re[i * 16 : i * 16 + 16, :] = summed[:, :128]
        tot_im[i * 16 : i * 16 + 16, :] = summed[:, 128:]

    flat_zero = jnp.zeros((PAIRS, 128), F32)
    flat_one = jnp.ones((PAIRS, 128), F32)
    state = (flat_zero, flat_zero)
    for c in range(CHUNKS):
        at = pl.ds(c, PAIRS, stride=CHUNKS)
        ent_re[at, :] = state[0]
        ent_im[at, :] = state[1]
        e = decay[c]
        state = cmul(
            (state[0] + tot_re[at, :], state[1] + tot_im[at, :]), (a_seg[0] * e, a_seg[1] * e)
        )
    l_buf[m, 0] = state[0].astype(BF16)
    l_buf[m, 1] = state[1].astype(BF16)
    for k in range(plane):
        when(m != k, plane_copy(l_buf, l_send, l_recv, k).start)

    l_k.wait()
    l_v.wait()
    kv_ref[WINDOW:, :] = dot(h_ref[...], wkv[...]).astype(BF16)
    halo = remote(
        kv_ref.at[TOK : TOK + WINDOW, :],
        kv_ref.at[0:WINDOW, :],
        halo_sem.at[0],
        halo_sem.at[1],
        (lax.rem(sp + 1, nz * plane), tp),
    )
    l_q.wait()
    q_ref[...] = dot(h_ref[...], wq[...]).astype(BF16).astype(F32) * 0.125
    when(crosses, pl.semaphore_wait, ready_halo, 1)
    pl.when(sp < nz * plane - 1)(halo.start)

    l_hg.wait()
    hg_ref[...] = jax.nn.sigmoid(dot(h_ref[...], whg[...]).astype(BF16).astype(F32))
    l_sg.wait()
    sg_ref[...] = jax.nn.sigmoid(dot(h_ref[...], wsg[...]).astype(BF16).astype(F32))

    cmat[...] = jnp.zeros_like(cmat)
    mmat[...] = jnp.zeros_like(mmat)
    for i in range(PAIRS):
        first = (i % 8) * 32
        value = [jnp.concatenate([t[2 * i], t[2 * i + 1]], axis=1) for t in (out_re, out_im)]
        value[1] = -value[1]
        for part in (0, 1):
            cols = slice(part * 128, part * 128 + 128)
            upper, lower = jnp.where(low, value[part], 0.0), jnp.where(low, 0.0, value[part])
            c_ref[i * 32 : i * 32 + 16, cols] = upper
            c_ref[i * 32 + 16 : i * 32 + 32, cols] = lower
            cols = slice(i * 256 + part * 128, i * 256 + part * 128 + 128)
            cmat[first : first + 16, cols] = upper.astype(BF16)
            cmat[first + 16 : first + 32, cols] = lower.astype(BF16)
    channel = lax.broadcasted_iota(jnp.int32, (2 * PAIRS, 512), 1)
    group = lax.broadcasted_iota(jnp.int32, (2 * PAIRS, 512), 0)
    spread = (channel // 16 == group).astype(F32).astype(BF16)
    rest = skip_t[...]
    spread_skip = jnp.zeros((16, 512), F32)
    for _ in range(3):
        part = rest.astype(BF16)
        spread_skip = spread_skip + dot(part, spread)
        rest = rest - part.astype(F32)
    skip = jnp.sum(
        jnp.where((channel % 16 == group)[:16], spread_skip, 0.0), axis=0, keepdims=True
    )
    for half in (0, 1):
        for k in range(8):
            i = 8 * half + k
            narrow = slice(i * 128, i * 128 + 128)
            summed = dot(tri[0:TOK, :], w_ref[:, i * 256 : i * 256 + 256])
            state = tuple(
                summed[:, 128 * part : 128 * part + 128].reshape(CHUNKS, SEG, 128)
                + entry[i * 16 : i * 16 + 16, :][:, None, :]
                for part, entry in ((0, ent_re), (1, ent_im))
            )
            state = cmul(state, (grow[0, :, narrow][None], grow[1, :, narrow][None]))
            s_ref[:, k * 256 : k * 256 + 128] = state[0].reshape(TOK, 128).astype(BF16)
            s_ref[:, k * 256 + 128 : k * 256 + 256] = state[1].reshape(TOK, 128).astype(BF16)
        cols = slice(half * 256, half * 256 + 256)
        rec = dot_nt(s_ref[...], cmat[:, half * 2048 : half * 2048 + 2048])
        yl_ref[:, cols] = rec * jnp.exp(es_ref[:, cols]) + skip[:, cols] * u_ref[:, cols]

    for k in range(plane):
        when(m != k, plane_wait, s_buf, s_send, s_recv, k)
        when(m != k, plane_wait, l_buf, l_send, l_recv, k)
    state, through = (flat_zero, flat_zero), (flat_one, flat_zero)
    before, before_through = state, through
    plane_shift = flat_zero
    for k in range(plane):
        here = m == k
        before = tuple(jnp.where(here, new, old) for new, old in zip(state, before))
        before_through = tuple(
            jnp.where(here, new, old) for new, old in zip(through, before_through)
        )
        e = jnp.exp(s_buf[k])
        factor = (a_dev[0] * e, a_dev[1] * e)
        through = cmul(factor, through)
        state = cmul(factor, state)
        state = (state[0] + l_buf[k, 0].astype(F32), state[1] + l_buf[k, 1].astype(F32))
        plane_shift = plane_shift + s_buf[k]
    zs_buf[z] = plane_shift
    zl_buf[z, 0] = state[0].astype(BF16)
    zl_buf[z, 1] = state[1].astype(BF16)
    when(z < nz - 1, pl.semaphore_wait, ready_z, nz - 1 - z)

    def z_copy(buf, send, recv, k):
        return remote(buf.at[z], buf.at[z], send.at[k], recv.at[z], (k * plane + m, tp))

    def z_wait(buf, send, recv, k):
        remote(buf.at[k], buf.at[k], send.at[k], recv.at[k], (k * plane + m, tp)).wait_recv()

    for k in range(nz - 1, 0, -1):
        when(z < k, z_copy(zl_buf, zl_send, zl_recv, k).start)
        when(z < k, z_copy(zs_buf, zs_send, zs_recv, k).start)

    seg_power = (flat_one, flat_zero)
    for c in range(CHUNKS):
        at = pl.ds(c, PAIRS, stride=CHUNKS)
        pow_re[at, :] = seg_power[0]
        pow_im[at, :] = seg_power[1]
        seg_power = cmul(seg_power, a_seg)
    for i in range(PAIRS):
        narrow = slice(i * 128, i * 128 + 128)
        start = (pow_re[i * 16 : i * 16 + 16, :][:, None, :], pow_im[i * 16 : i * 16 + 16, :][:, None, :])
        value = cmul(start, (grow[0, :, narrow][None], grow[1, :, narrow][None]))
        for part in (0, 1):
            cols = slice(i * 256 + part * 128, i * 256 + part * 128 + 128)
            g_ref[:, cols] = value[part].reshape(TOK, 128).astype(BF16)
    ed_ref[...] = jnp.exp(shift_sums((col <= row).astype(F32).astype(BF16)))

    @pl.when(sp == 0)
    def _():
        kv_ref[0:WINDOW, :] = jnp.zeros((WINDOW, 512), BF16)

    pl.when(sp > 0)(halo.wait_recv)
    qi = lax.rem(lax.broadcasted_iota(jnp.int32, (2 * WINDOW, 2 * WINDOW), 0), WINDOW)
    key_at = lax.broadcasted_iota(jnp.int32, (2 * WINDOW, 2 * WINDOW), 1)
    inside = (key_at > qi) & (key_at <= qi + WINDOW)
    left = lax.broadcasted_iota(jnp.int32, (WINDOW, 128), 1) < 64
    for n in range(TOK // WINDOW):
        allowed = inside & ((key_at >= WINDOW) | (sp > 0)) if n == 0 else inside
        rows = slice(n * WINDOW, (n + 1) * WINDOW)
        keys = slice(n * WINDOW, (n + 2) * WINDOW)
        for h in range(KV_HEADS):
            q = q_ref[rows, h * 128 : h * 128 + 128]
            turned = pltpu.roll(q, 64, 1)
            in_half = left if h % 2 == 0 else jnp.logical_not(left)
            first, second = (q, turned) if h % 2 == 0 else (turned, q)
            stacked = jnp.concatenate(
                [jnp.where(in_half, part, 0.0).astype(BF16) for part in (first, second)], axis=0
            )
            tile = slice((h // 2) * 128, (h // 2) * 128 + 128)
            scores = dot_nt(stacked, kv_ref[keys, tile])
            scores = jnp.where(allowed, scores, -1e30)
            first_row = lax.broadcasted_iota(jnp.int32, (2 * WINDOW, 1), 0) < WINDOW
            sink_col = jnp.where(first_row, sink[2 * h], sink[2 * h + 1])
            peak = jnp.maximum(jnp.max(scores, axis=1, keepdims=True), sink_col)
            e = jnp.exp(scores - peak)
            total = jnp.sum(e, axis=1, keepdims=True) + jnp.exp(sink_col - peak)
            vtile = slice(256 + (h // 2) * 128, 256 + (h // 2) * 128 + 128)
            mixed = dot(e.astype(BF16), kv_ref[keys, vtile]) / total
            a, b = mixed[:WINDOW], mixed[WINDOW:]
            if h % 2 == 0:
                joined = jnp.where(left, a, pltpu.roll(b, 64, 1))
            else:
                joined = jnp.where(left, pltpu.roll(a, 64, 1), b)
            gate = hg_ref[rows, h * 128 : h * 128 + 128]
            hm_ref[rows, h * 128 : h * 128 + 128] = (gate * joined).astype(BF16)
    l_ho.wait()
    acc_ref[...] = dot(hm_ref[...], who[...])

    pre[...] = jnp.zeros_like(pre)
    for k in range(nz - 1):

        @pl.when(k < z)
        def _(k=k):
            z_wait(zs_buf, zs_send, zs_recv, k)
            z_wait(zl_buf, zl_send, zl_recv, k)
            e = jnp.exp(zs_buf[k])
            new = cmul((a_plane[0] * e, a_plane[1] * e), (pre[0], pre[1]))
            pre[0] = new[0] + zl_buf[k, 0].astype(F32)
            pre[1] = new[1] + zl_buf[k, 1].astype(F32)

    carry = cmul(before_through, (pre[0], pre[1]))
    carry = (before[0] + carry[0], before[1] + carry[1])
    for i in range(PAIRS):
        first = (i % 8) * 32
        value = (c_ref[i * 32 : i * 32 + 32, 0:128], c_ref[i * 32 : i * 32 + 32, 128:256])
        value = cmul(value, (carry[0][i : i + 1, :], -carry[1][i : i + 1, :]))
        for part in (0, 1):
            cols = slice(i * 256 + part * 128, i * 256 + part * 128 + 128)
            mmat[first : first + 32, cols] = value[part].astype(BF16)
    for half in (0, 1):
        cols = slice(half * 256, half * 256 + 256)
        wide = slice(half * 2048, half * 2048 + 2048)
        rec = dot_nt(g_ref[:, wide], mmat[:, wide])
        rec = rec * ed_ref[:, cols] + yl_ref[:, cols]
        sm_ref[:, cols] = (sg_ref[:, cols] * jax.nn.gelu(rec)).astype(BF16)

    l_so.wait()
    outs = []
    for k in range(N_OUT):
        cols = pl.ds(pl.multiple_of(other * HALF + k * 256, 256), 256)
        psend[k] = (acc_ref[:, cols] + dot(sm_ref[...], wso[:, cols])).astype(BF16)
        copy = remote(psend.at[k], precv.at[k], out_send.at[k], out_recv.at[k], (sp, other))
        copy.start()
        outs.append(copy)
    for k in range(N_OUT):
        cols = pl.ds(pl.multiple_of(tp * HALF + k * 256, 256), 256)
        own = acc_ref[:, cols] + dot(sm_ref[...], wso[:, cols])
        outs[k].wait_recv()
        out[:, k * 256 : k * 256 + 256] = (own + precv[k].astype(F32)).astype(BF16)

    send_h.wait_send()
    pl.when(sp < nz * plane - 1)(halo.wait_send)
    for copy in outs:
        copy.wait_send()
    for k in range(plane):
        when(m != k, plane_copy(s_buf, s_send, s_recv, k).wait_send)
        when(m != k, plane_copy(l_buf, l_send, l_recv, k).wait_send)
    for k in range(1, nz):
        when(z < k, z_copy(zs_buf, zs_send, zs_recv, k).wait_send)
        when(z < k, z_copy(zl_buf, zl_send, zl_recv, k).wait_send)


def on_device(
    sizes,
    hidden,
    query_weight,
    key_weight,
    value_weight,
    head_gate_weight,
    state_in_weight,
    state_gate_weight,
    sink_logit,
    decay_real,
    decay_frequency,
    log_step,
    input_real,
    input_imaginary,
    output_real,
    output_imaginary,
    skip_weight,
    decay_shift,
    head_out_weight,
    state_out_weight,
):
    nz, ny, nx = sizes
    vmem = pl.BlockSpec(memory_space=pltpu.VMEM)
    hbm = pl.BlockSpec(memory_space=pl.ANY)
    plane = ny * nx
    scratch = [
        ((2 * PAIRS, 64), F32),
        ((2 * PAIRS, 64), F32),
        ((2 * PAIRS, 16, 64), F32),
        ((2 * PAIRS, 16, 64), F32),
        ((2 * PAIRS, 16, 64), F32),
        ((2 * PAIRS, 16, 64), F32),
        ((16, 2 * PAIRS), F32),
        ((2 * PAIRS, TOK), F32),
        ((TOK, D), BF16),
        ((D, 512), BF16),
        ((D, 512), BF16),
        ((D, 512), BF16),
        ((D, 512), BF16),
        ((D, 512), BF16),
        ((512, D), BF16),
        ((512, D), BF16),
        ((128, LANES), BF16),
        ((256, LANES), BF16),
        ((256, LANES), BF16),
        ((512, 256), F32),
        ((TOK + CHUNKS, TOK), BF16),
        ((2, SEG, PAIRS * 128), F32),
        ((2, SEG, PAIRS * 128), F32),
        ((CHUNKS, PAIRS, 128), F32),
        ((2 * PAIRS, 128), F32),
        ((TOK, 512), F32),
        ((TOK, 512), BF16),
        ((TOK, 512), F32),
        ((TOK, 512), F32),
        ((TOK, LANES), BF16),
        ((TOK, LANES // 2), BF16),
        ((TOK, LANES), BF16),
        ((TOK, 512), F32),
        ((PAIRS * CHUNKS, 128), F32),
        ((PAIRS * CHUNKS, 128), F32),
        ((PAIRS * CHUNKS, 128), F32),
        ((PAIRS * CHUNKS, 128), F32),
        ((PAIRS * CHUNKS, 128), F32),
        ((PAIRS * CHUNKS, 128), F32),
        ((TOK, 512), F32),
        ((TOK + WINDOW, 512), BF16),
        ((TOK, 512), F32),
        ((TOK, 512), F32),
        ((TOK, 512), BF16),
        ((TOK, 512), BF16),
        ((TOK, D), F32),
        ((N_OUT, TOK, 256), BF16),
        ((N_OUT, TOK, 256), BF16),
        ((plane, PAIRS, 128), F32),
        ((plane, 2, PAIRS, 128), BF16),
        ((nz, PAIRS, 128), F32),
        ((nz, 2, PAIRS, 128), BF16),
        ((2, PAIRS, 128), F32),
    ]
    dma = pltpu.SemaphoreType.DMA
    regular = pltpu.SemaphoreType.REGULAR
    return pl.pallas_call(
        functools.partial(kernel, sizes),
        out_shape=jax.ShapeDtypeStruct((TOK, HALF), BF16),
        in_specs=[hbm] * 19,
        out_specs=vmem,
        scratch_shapes=[pltpu.SMEM((8,), F32), pltpu.SMEM((2 * PAIRS,), F32)]
        + [pltpu.VMEM(shape, dtype) for shape, dtype in scratch]
        + [dma((19,)), dma((2,)), dma((2,)), dma((N_OUT,)), dma((N_OUT,))]
        + [dma((plane,))] * 4
        + [dma((nz,))] * 4
        + [regular] * 3,
        compiler_params=pltpu.CompilerParams(
            collective_id=0, has_side_effects=True, vmem_limit_bytes=60 * 1024 * 1024
        ),
        name="layer",
    )(
        hidden,
        query_weight,
        key_weight,
        value_weight,
        head_gate_weight,
        state_in_weight,
        state_gate_weight,
        head_out_weight,
        state_out_weight,
        sink_logit,
        log_step,
        decay_real,
        decay_frequency,
        input_real.transpose(0, 2, 1),
        input_imaginary.transpose(0, 2, 1),
        output_real,
        output_imaginary,
        skip_weight.T,
        decay_shift,
    )


def solution(mesh):
    sizes = SP_SIZES[mesh.shape["sp"]]
    in_specs = (
        P("sp", "tp"),
        P(None, "tp"),
        P(None, "tp"),
        P(None, "tp"),
        P(None, "tp"),
        P(None, "tp"),
        P(None, "tp"),
        P("tp"),
        P("tp", None),
        P("tp", None),
        P("tp"),
        P("tp", None, None),
        P("tp", None, None),
        P("tp", None, None),
        P("tp", None, None),
        P("tp", None),
        P("tp", "sp"),
        P("tp", None),
        P("tp", None),
    )
    return jax.shard_map(
        functools.partial(on_device, sizes),
        mesh=mesh,
        in_specs=in_specs,
        out_specs=P("sp", "tp"),
        check_vma=False,
    )
```

time: 44.1 us -> 29.6 us (0.67)
  the two profiles are of different devices: /device:TPU:193 before, /device:TPU:41 now
where the time goes in v2:
time: 29.6 us; the launch traced here: 29.5 us
  Pallas kernels  27.6 us (93%)
  local copies, waits for them, and re-layouts  1.87 us (6%)
    pallas_call x1, Pallas kernels, on_device(): pl.pallas_call(functools.partial(kernel, sizes), out_shape=jax.ShapeDtype...  27.6 us
    unnamed x1, local copies, waits for them, and re-layouts  1.87 us

profile of v2, /device:TPU:41, one launch (start us, length us, event | category | flops | bytes accessed | tf_op | source)
XLA Modules:
  0.0 29.5 jit_solution(11302161471874245164)
XLA Ops:
  0.0 27.6 %layer.1 = bf16[256,1024]{1,0:T(8,128)(2,1)} custom-call(bf16[256,1024]{1,0:T(8,128)(2,1)} %refs_0_.1, bf16[2048,512]{1,0:T(8,128)(2,1)} %refs_1_.1, bf16[2048,256]{1,0:T(8,128)(2,1)} %refs_2_.1, bf16[2048,256]{1,0:T(8,128)(2,1)} %refs_3_.1, bf16[2048,512]{1,0:T(8,128)(2,1)} %refs_4_.1, bf16[2048,512]{1,0:T(8,128)(2,1)} %refs_5_.1, ...), custom_call_target="tpu_custom_call" | custom-call | tf_op jit(solution)/shard_map/layer/pallas_call | solution.py:650
  27.6 1.9 %copy.21 = bf16[256,1024]{1,0:T(8,128)(2,1)} copy(bf16[256,1024]{1,0:T(8,128)(2,1)} %layer.1) | data formatting | bytes 1048576

commit v3 on v2

v3 whole, which is shorter than its diff:
```python
import functools

import jax
import jax.numpy as jnp
from jax import lax
from jax.experimental import pallas as pl
from jax.experimental.pallas import tpu as pltpu
from jax.sharding import PartitionSpec as P

MESH = pl.DeviceIdType.MESH
F32 = jnp.float32
BF16 = jnp.bfloat16

TOK = 256
D = 2048
HALF = D // 2
WINDOW = 128
SEG = 16
CHUNKS = TOK // SEG
PAIRS = 16
LANES = PAIRS * 256
KV_HEADS = 4
SP_SIZES = {128: (8, 4, 4), 8: (2, 2, 2)}

FAR = 3
N_OUT = 2


def dot(a, b):
    return jnp.dot(a, b, preferred_element_type=F32)


def dot_nt(a, b):
    return lax.dot_general(a, b, (((1,), (1,)), ((), ())), preferred_element_type=F32)


def cmul(a, b):
    return (a[0] * b[0] - a[1] * b[1], a[0] * b[1] + a[1] * b[0])


def csquares(a, times):
    for _ in range(times):
        a = cmul(a, a)
    return a


def log2(n):
    return n.bit_length() - 1


def kernel(sizes, *refs):
    nz, ny, nx = sizes
    plane = ny * nx
    (
        hidden,
        w_query,
        w_key,
        w_value,
        w_hgate,
        w_sin,
        w_sgate,
        w_hout,
        w_sout,
        sink_in,
        step_in,
        real_in,
        freq_in,
        in_re_in,
        in_im_in,
        out_re_in,
        out_im_in,
        skip_in,
        shift_in,
        out,
        sink,
        log_step,
        decay_real,
        decay_freq,
        in_re,
        in_im,
        out_re,
        out_im,
        skip_t,
        shift,
        h_ref,
        win,
        wkvq,
        wgate,
        who,
        wso,
        drive,
        cmat,
        skip_ref,
        bias,
        tri,
        grow,
        shrink,
        decay,
        pair_tile,
        u_ref,
        us_ref,
        es_ref,
        x_ref,
        s_ref,
        tot_re,
        tot_im,
        ent_re,
        ent_im,
        q_ref,
        kv_ref,
        hg_ref,
        sg_ref,
        hm_ref,
        sm_ref,
        acc_ref,
        psend,
        precv,
        s_buf,
        l_buf,
        zs_buf,
        zl_buf,
        pre,
        load_sem,
        h_sem,
        halo_sem,
        out_send,
        out_recv,
        s_send,
        s_recv,
        l_send,
        l_recv,
        zs_send,
        zs_recv,
        zl_send,
        zl_recv,
        ready_near,
        ready_far,
        ready_z,
    ) = refs
    sp, tp = lax.axis_index("sp"), lax.axis_index("tp")
    z, m = sp // plane, sp % plane
    other = 1 - tp

    apart = [k % nx + k // nx - (m % nx + m // nx) for k in range(plane)]
    behind = [
        jnp.logical_or(apart[k] > 0, jnp.logical_and(apart[k] == 0, k > m)) for k in range(plane)
    ]
    ahead = [
        jnp.logical_or(apart[k] < 0, jnp.logical_and(apart[k] == 0, k < m)) for k in range(plane)
    ]

    def count(conditions):
        return sum(condition.astype(jnp.int32) for condition in conditions)

    barrier = pltpu.get_barrier_semaphore()

    def signal(semaphore, device):
        pl.semaphore_signal(semaphore, inc=1, device_id=device, device_id_type=MESH)

    def when(condition, act, *args):
        pl.when(condition)(functools.partial(act, *args))

    crosses = jnp.logical_and(m == plane - 1, z < nz - 1)
    crossed = jnp.logical_and(m == 0, z > 0)
    signal(barrier, (sp, other))
    for k in range(plane):
        when(behind[k], signal, barrier, (z * plane + k, tp))
    for r in range(1, nz):
        when(z + r < nz, signal, barrier, (sp + r * plane, tp))
    when(crossed, signal, barrier, (sp - 1, tp))
    loads = []

    def load(src, dst):
        copy = pltpu.make_async_copy(src, dst, load_sem.at[len(loads)])
        copy.start()
        loads.append(copy)
        return copy

    def remote(src, dst, send, recv, device):
        return pltpu.make_async_remote_copy(
            src_ref=src,
            dst_ref=dst,
            send_sem=send,
            recv_sem=recv,
            device_id=device,
            device_id_type=MESH,
        )

    mine = pl.ds(pl.multiple_of(tp * HALF, HALF), HALF)
    theirs = pl.ds(pl.multiple_of(other * HALF, HALF), HALF)
    l_h = load(hidden, h_ref.at[:, mine])
    small = [
        load(src, dst)
        for src, dst in (
            (step_in, log_step),
            (real_in, decay_real),
            (freq_in, decay_freq),
            (shift_in, shift),
            (in_re_in, in_re),
            (in_im_in, in_im),
            (out_re_in, out_re),
            (out_im_in, out_im),
            (skip_in, skip_t),
            (sink_in, sink),
        )
    ]
    l_in = load(w_sin, win)

    pl.semaphore_wait(barrier, 1 + count(ahead) + z + count([crosses]))
    l_h.wait()
    send_h = remote(h_ref.at[:, mine], h_ref.at[:, mine], h_sem.at[0], h_sem.at[1], (sp, other))
    send_h.start()
    for k in range(plane):
        far = apart[k] <= -FAR
        when(far, signal, ready_far, (z * plane + k, tp))
        close = jnp.logical_and(ahead[k], jnp.logical_not(far))
        when(close, signal, ready_near, (z * plane + k, tp))
    for r in range(1, nz):
        when(z >= r, signal, ready_z, (sp - r * plane, tp))
    l_k = load(w_key, wkvq.at[:, 0:256])
    l_v = load(w_value, wkvq.at[:, 256:512])
    l_q = load(w_query, wkvq.at[:, 512:1024])

    for copy in small:
        copy.wait()
    low = lax.broadcasted_iota(jnp.int32, (PAIRS, 128), 1) < 64

    def paired(value):
        pair_tile[...] = jnp.concatenate([value, value], axis=1)
        even = pair_tile[pl.ds(0, PAIRS, stride=2), :]
        odd = pair_tile[pl.ds(1, PAIRS, stride=2), :]
        return jnp.where(low, even, odd)

    pair_row = lax.broadcasted_iota(jnp.int32, (PAIRS, 128), 0)
    step = jnp.zeros((PAIRS, 128), F32)
    for i in range(PAIRS):
        step = jnp.where(
            pair_row == i, jnp.where(low, log_step[2 * i], log_step[2 * i + 1]), step
        )
    step = jnp.exp(step)
    real, freq = paired(decay_real[...]), paired(decay_freq[...])
    magnitude, inverse = jnp.exp(real * step), jnp.exp(-(real * step))
    cosine, sine = jnp.cos(freq * step), jnp.sin(freq * step)
    base = (magnitude * cosine, magnitude * sine)
    base_inv = (inverse * cosine, -(inverse * sine))
    denominator = real * real + freq * freq
    less = base[0] - 1.0
    zoh = (
        (less * real + base[1] * freq) / denominator,
        (base[1] * real - less * freq) / denominator,
    )

    row = lax.broadcasted_iota(jnp.int32, (TOK, TOK), 0)
    col = lax.broadcasted_iota(jnp.int32, (TOK, TOK), 1)
    tri[0:TOK, :] = ((row // SEG == col // SEG) & (col <= row)).astype(F32).astype(BF16)
    srow = lax.broadcasted_iota(jnp.int32, (CHUNKS, TOK), 0)
    scol = lax.broadcasted_iota(jnp.int32, (CHUNKS, TOK), 1)
    tri[TOK:, :] = (scol // SEG == srow).astype(F32).astype(BF16)
    drive[...] = jnp.zeros_like(drive)
    for i in range(PAIRS):
        factor = (zoh[0][i : i + 1, :], zoh[1][i : i + 1, :])
        first = (i % 4) * 32
        value = cmul(factor, tuple(jnp.concatenate([t[2 * i], t[2 * i + 1]], axis=1) for t in (in_re, in_im)))
        for part in (0, 1):
            cols = slice(i * 256 + part * 128, i * 256 + part * 128 + 128)
            drive[first : first + 16, cols] = jnp.where(low, value[part], 0.0).astype(BF16)
            drive[first + 16 : first + 32, cols] = jnp.where(low, 0.0, value[part]).astype(BF16)

    cmat[...] = jnp.zeros_like(cmat)
    for i in range(PAIRS):
        first = (i % 8) * 32
        value = [jnp.concatenate([t[2 * i], t[2 * i + 1]], axis=1) for t in (out_re, out_im)]
        value[1] = -value[1]
        for part in (0, 1):
            cols = slice(i * 256 + part * 128, i * 256 + part * 128 + 128)
            cmat[first : first + 16, cols] = jnp.where(low, value[part], 0.0).astype(BF16)
            cmat[first + 16 : first + 32, cols] = jnp.where(low, 0.0, value[part]).astype(BF16)
    channel = lax.broadcasted_iota(jnp.int32, (2 * PAIRS, 512), 1)
    group = lax.broadcasted_iota(jnp.int32, (2 * PAIRS, 512), 0)
    spread = (channel // 16 == group).astype(F32).astype(BF16)
    rest = skip_t[...]
    spread_skip = jnp.zeros((16, 512), F32)
    for _ in range(3):
        part = rest.astype(BF16)
        spread_skip = spread_skip + dot(part, spread)
        rest = rest - part.astype(F32)
    skip_ref[...] = jnp.sum(
        jnp.where((channel % 16 == group)[:16], spread_skip, 0.0), axis=0, keepdims=True
    )
    qi = lax.rem(row, WINDOW)
    inside = (col > qi) & (col <= qi + WINDOW)
    bias[0] = jnp.where(inside & ((col >= WINDOW) | (sp > 0)), 0.0, -1e30)
    bias[1] = jnp.where(inside, 0.0, -1e30)

    power = lax.broadcasted_iota(jnp.int32, (8, 128), 0) + 1
    ones, zeros = jnp.ones((8, 128), F32), jnp.zeros((8, 128), F32)
    for table, root in ((grow, base), (shrink, base_inv)):
        for i in range(PAIRS):
            b = tuple(jnp.broadcast_to(part[i : i + 1, :], (8, 128)) for part in root)
            value = (ones, zeros)
            for bit in range(4):
                has = (power >> bit) & 1 == 1
                value = cmul(value, (jnp.where(has, b[0], ones), jnp.where(has, b[1], zeros)))
                if bit < 3:
                    b = cmul(b, b)
            cols = slice(i * 128, i * 128 + 128)
            upper = cmul(value, b)
            for k in (0, 1):
                table[k, 0:8, cols] = value[k]
                table[k, 8:16, cols] = upper[k]
    a_seg = csquares(base, log2(SEG))
    a_dev = csquares(a_seg, log2(CHUNKS))
    a_plane = csquares(a_dev, log2(plane))

    def shift_sums(mask):
        rest = jnp.broadcast_to(shift[...][:, None, :], (2 * PAIRS, 16, TOK)).reshape(512, TOK)
        sums = None
        for _ in range(3):
            part = rest.astype(BF16)
            term = dot_nt(mask, part)
            sums = term if sums is None else sums + term
            rest = rest - part.astype(F32)
        return sums

    es_ref[...] = shift_sums(tri[0:TOK, :])
    lane = lax.broadcasted_iota(jnp.int32, (PAIRS, 128), 1)
    total_shift = jnp.zeros((PAIRS, 128), F32)
    for c in range(CHUNKS):
        if c % 8 == 0:
            pair_tile[...] = shift[:, c * SEG : c * SEG + 128]
            even = pair_tile[pl.ds(0, PAIRS, stride=2), :]
            odd = pair_tile[pl.ds(1, PAIRS, stride=2), :]
        inside = lane // SEG == c % 8
        s = jnp.where(
            low,
            jnp.sum(jnp.where(inside, even, 0.0), axis=1, keepdims=True),
            jnp.sum(jnp.where(inside, odd, 0.0), axis=1, keepdims=True),
        )
        total_shift = total_shift + s
        decay[c] = jnp.exp(s)
    s_buf[m] = jnp.sum(
        jnp.where(lane % 64 == pair_row, total_shift, 0.0), axis=0, keepdims=True
    )

    l_in.wait()
    u_ref[...] = dot(h_ref[:, mine], win[mine, :])
    send_h.wait_recv()
    l_hg = load(w_hgate, wgate.at[:, 0:512])
    l_sg = load(w_sgate, wgate.at[:, 512:1024])
    l_ho = load(w_hout, who)
    l_so = load(w_sout, wso)
    row_end = m % nx == nx - 1
    l_k.wait()
    l_v.wait()
    halo = remote(
        kv_ref.at[TOK : TOK + WINDOW, :],
        kv_ref.at[0:WINDOW, :],
        halo_sem.at[0],
        halo_sem.at[1],
        (lax.rem(sp + 1, nz * plane), tp),
    )

    @pl.when(row_end)
    def _():
        kv_ref[TOK:, :] = dot(h_ref[WINDOW:, :], wkvq[:, 0:512]).astype(BF16)

    u = (u_ref[...] + dot(h_ref[:, theirs], win[theirs, :])).astype(BF16).astype(F32)
    u_ref[...] = u
    us_ref[...] = (u * jnp.exp(-es_ref[...])).astype(BF16)
    pl.when(jnp.logical_and(row_end, sp < nz * plane - 1))(halo.start)

    def plane_copy(buf, send, recv, k):
        return remote(buf.at[m], buf.at[m], send.at[k], recv.at[m], (z * plane + k, tp))

    def plane_wait(buf, send, recv, k):
        remote(buf.at[k], buf.at[k], send.at[k], recv.at[k], (z * plane + k, tp)).wait_recv()

    for i in range(PAIRS):
        cols, narrow = slice(i * 256, i * 256 + 256), slice(i * 128, i * 128 + 128)
        j = i // 4
        push = dot(us_ref[:, j * 128 : j * 128 + 128], drive[:, cols])
        push = (push[:, :128].reshape(CHUNKS, SEG, 128), push[:, 128:].reshape(CHUNKS, SEG, 128))
        back = (shrink[0, :, narrow][None], shrink[1, :, narrow][None])
        w = cmul(push, back)
        w = jnp.concatenate([part.reshape(TOK, 128).astype(BF16) for part in w], axis=1)
        summed = dot(tri[...], w)
        x_ref[:, cols] = summed[:TOK]
        tot_re[i * 16 : i * 16 + 16, :] = summed[TOK:, :128]
        tot_im[i * 16 : i * 16 + 16, :] = summed[TOK:, 128:]

    flat_zero = jnp.zeros((PAIRS, 128), F32)
    flat_one = jnp.ones((PAIRS, 128), F32)

    def chunk_scan(state, keep):
        for c in range(CHUNKS):
            at = pl.ds(c, PAIRS, stride=CHUNKS)
            if keep:
                ent_re[at, :] = state[0]
                ent_im[at, :] = state[1]
            e = decay[c]
            state = cmul(
                (state[0] + tot_re[at, :], state[1] + tot_im[at, :]), (a_seg[0] * e, a_seg[1] * e)
            )
        return state

    state = chunk_scan((flat_zero, flat_zero), False)
    l_buf[m, 0] = state[0].astype(BF16)
    l_buf[m, 1] = state[1].astype(BF16)
    def send_to(k, condition):
        when(condition, plane_copy(l_buf, l_send, l_recv, k).start)
        when(condition, plane_copy(s_buf, s_send, s_recv, k).start)

    near = [jnp.logical_and(behind[k], apart[k] < FAR) for k in range(plane)]
    far = [apart[k] >= FAR for k in range(plane)]
    for k in range(plane):
        send_to(k, ahead[k])
    when(count(near) > 0, pl.semaphore_wait, ready_near, jnp.maximum(count(near), 1))
    for k in range(plane):
        send_to(k, near[k])

    l_q.wait()
    rows = dot(h_ref[...], wkvq[...]).astype(BF16)
    kv_ref[WINDOW:TOK, :] = rows[0:WINDOW, 0:512]
    q_ref[...] = rows[:, 512:1024].astype(F32) * 0.125

    @pl.when(jnp.logical_not(row_end))
    def _():
        kv_ref[TOK:, :] = rows[WINDOW:, 0:512]

    pl.when(jnp.logical_not(row_end))(halo.start)
    when(count(far) > 0, pl.semaphore_wait, ready_far, jnp.maximum(count(far), 1))
    for k in range(plane):
        send_to(k, far[k])

    l_hg.wait()
    l_sg.wait()
    gates = jax.nn.sigmoid(dot(h_ref[...], wgate[...]).astype(BF16).astype(F32))
    hg_ref[...] = gates[:, 0:512]
    sg_ref[...] = gates[:, 512:1024]

    left = lax.broadcasted_iota(jnp.int32, (WINDOW, 128), 1) < 64

    def attend(n):
        rows = slice(n * WINDOW, (n + 1) * WINDOW)
        keys = slice(n * WINDOW, (n + 2) * WINDOW)
        for h in range(KV_HEADS):
            q = q_ref[rows, h * 128 : h * 128 + 128]
            turned = pltpu.roll(q, 64, 1)
            in_half = left if h % 2 == 0 else jnp.logical_not(left)
            first, second = (q, turned) if h % 2 == 0 else (turned, q)
            stacked = jnp.concatenate(
                [jnp.where(in_half, part, 0.0).astype(BF16) for part in (first, second)], axis=0
            )
            tile = slice((h // 2) * 128, (h // 2) * 128 + 128)
            scores = dot_nt(stacked, kv_ref[keys, tile]) + bias[n]
            first_row = lax.broadcasted_iota(jnp.int32, (2 * WINDOW, 1), 0) < WINDOW
            sink_col = jnp.where(first_row, sink[2 * h], sink[2 * h + 1])
            peak = jnp.maximum(jnp.max(scores, axis=1, keepdims=True), sink_col)
            e = jnp.exp(scores - peak)
            total = jnp.sum(e, axis=1, keepdims=True) + jnp.exp(sink_col - peak)
            vtile = slice(256 + (h // 2) * 128, 256 + (h // 2) * 128 + 128)
            mixed = dot(e.astype(BF16), kv_ref[keys, vtile]) / total
            a, b = mixed[:WINDOW], mixed[WINDOW:]
            if h % 2 == 0:
                joined = jnp.where(left, a, pltpu.roll(b, 64, 1))
            else:
                joined = jnp.where(left, pltpu.roll(a, 64, 1), b)
            gate = hg_ref[rows, h * 128 : h * 128 + 128]
            hm_ref[rows, h * 128 : h * 128 + 128] = (gate * joined).astype(BF16)
    attend(1)

    for k in range(plane):
        when(m != k, plane_wait, s_buf, s_send, s_recv, k)
        when(m != k, plane_wait, l_buf, l_send, l_recv, k)
    state, through = (flat_zero, flat_zero), (flat_one, flat_zero)
    before, before_through = state, through
    plane_shift = jnp.zeros((1, 128), F32)

    def spread_row(sums):
        own = jnp.where(lane % 64 == pair_row, sums, 0.0)
        return jnp.where(
            low,
            jnp.sum(jnp.where(low, own, 0.0), axis=1, keepdims=True),
            jnp.sum(jnp.where(low, 0.0, own), axis=1, keepdims=True),
        )

    for k in range(plane):
        here = m == k
        before = tuple(jnp.where(here, new, old) for new, old in zip(state, before))
        before_through = tuple(
            jnp.where(here, new, old) for new, old in zip(through, before_through)
        )
        e = jnp.exp(spread_row(s_buf[k]))
        factor = (a_dev[0] * e, a_dev[1] * e)
        through = cmul(factor, through)
        state = cmul(factor, state)
        state = (state[0] + l_buf[k, 0].astype(F32), state[1] + l_buf[k, 1].astype(F32))
        plane_shift = plane_shift + s_buf[k]
    zs_buf[z] = plane_shift
    zl_buf[z, 0] = state[0].astype(BF16)
    zl_buf[z, 1] = state[1].astype(BF16)
    when(z < nz - 1, pl.semaphore_wait, ready_z, nz - 1 - z)

    def z_copy(buf, send, recv, k):
        return remote(buf.at[z], buf.at[z], send.at[k], recv.at[z], (k * plane + m, tp))

    def z_wait(buf, send, recv, k):
        remote(buf.at[k], buf.at[k], send.at[k], recv.at[k], (k * plane + m, tp)).wait_recv()

    for k in range(nz - 1, 0, -1):
        when(z < k, z_copy(zl_buf, zl_send, zl_recv, k).start)
        when(z < k, z_copy(zs_buf, zs_send, zs_recv, k).start)

    l_ho.wait()

    @pl.when(sp == 0)
    def _():
        kv_ref[0:WINDOW, :] = jnp.zeros((WINDOW, 512), BF16)

    pl.when(sp > 0)(halo.wait_recv)
    attend(0)
    acc_ref[...] = dot(hm_ref[...], who[...])

    pre[...] = jnp.zeros_like(pre)
    for k in range(nz - 1):

        @pl.when(k < z)
        def _(k=k):
            z_wait(zs_buf, zs_send, zs_recv, k)
            z_wait(zl_buf, zl_send, zl_recv, k)
            e = jnp.exp(spread_row(zs_buf[k]))
            new = cmul((a_plane[0] * e, a_plane[1] * e), (pre[0], pre[1]))
            pre[0] = new[0] + zl_buf[k, 0].astype(F32)
            pre[1] = new[1] + zl_buf[k, 1].astype(F32)

    carry = cmul(before_through, (pre[0], pre[1]))
    carry = (before[0] + carry[0], before[1] + carry[1])
    chunk_scan(carry, True)
    for half in (0, 1):
        for k in range(8):
            i = 8 * half + k
            narrow = slice(i * 128, i * 128 + 128)
            growth = (grow[0, :, narrow], grow[1, :, narrow])
            for c in range(CHUNKS):
                rows = slice(c * SEG, c * SEG + SEG)
                entry = i * CHUNKS + c
                re, im = slice(i * 256, i * 256 + 128), slice(i * 256 + 128, i * 256 + 256)
                state = (
                    x_ref[rows, re] + ent_re[entry : entry + 1, :],
                    x_ref[rows, im] + ent_im[entry : entry + 1, :],
                )
                state = cmul(state, growth)
                s_ref[rows, re] = state[0].astype(BF16)
                s_ref[rows, im] = state[1].astype(BF16)
        cols = slice(half * 256, half * 256 + 256)
        wide = slice(half * 2048, half * 2048 + 2048)
        rec = dot_nt(s_ref[:, wide], cmat[:, wide])
        rec = rec * jnp.exp(es_ref[:, cols]) + skip_ref[:, cols] * u_ref[:, cols]
        sm_ref[:, cols] = (sg_ref[:, cols] * jax.nn.gelu(rec)).astype(BF16)

    l_so.wait()
    outs = []
    width = HALF // N_OUT
    for k in range(N_OUT):
        cols = pl.ds(pl.multiple_of(other * HALF + k * width, width), width)
        psend[k] = (acc_ref[:, cols] + dot(sm_ref[...], wso[:, cols])).astype(BF16)
        copy = remote(psend.at[k], precv.at[k], out_send.at[k], out_recv.at[k], (sp, other))
        copy.start()
        outs.append(copy)
    acc_ref[:, mine] = acc_ref[:, mine] + dot(sm_ref[...], wso[:, mine])
    for k in range(N_OUT):
        cols = pl.ds(pl.multiple_of(tp * HALF + k * width, width), width)
        outs[k].wait_recv()
        out[:, k * width : k * width + width] = (acc_ref[:, cols] + precv[k].astype(F32)).astype(BF16)

    send_h.wait_send()
    pl.when(sp < nz * plane - 1)(halo.wait_send)
    for copy in outs:
        copy.wait_send()
    for k in range(plane):
        when(m != k, plane_copy(s_buf, s_send, s_recv, k).wait_send)
        when(m != k, plane_copy(l_buf, l_send, l_recv, k).wait_send)
    for k in range(1, nz):
        when(z < k, z_copy(zs_buf, zs_send, zs_recv, k).wait_send)
        when(z < k, z_copy(zl_buf, zl_send, zl_recv, k).wait_send)


def on_device(
    sizes,
    hidden,
    query_weight,
    key_weight,
    value_weight,
    head_gate_weight,
    state_in_weight,
    state_gate_weight,
    sink_logit,
    decay_real,
    decay_frequency,
    log_step,
    input_real,
    input_imaginary,
    output_real,
    output_imaginary,
    skip_weight,
    decay_shift,
    head_out_weight,
    state_out_weight,
):
    nz, ny, nx = sizes
    vmem = pl.BlockSpec(memory_space=pltpu.VMEM)
    hbm = pl.BlockSpec(memory_space=pl.ANY)
    plane = ny * nx
    scratch = [
        ((2 * PAIRS, 64), F32),
        ((2 * PAIRS, 64), F32),
        ((2 * PAIRS, 16, 64), F32),
        ((2 * PAIRS, 16, 64), F32),
        ((2 * PAIRS, 16, 64), F32),
        ((2 * PAIRS, 16, 64), F32),
        ((16, 2 * PAIRS), F32),
        ((2 * PAIRS, TOK), F32),
        ((TOK, D), BF16),
        ((D, 512), BF16),
        ((D, 1024), BF16),
        ((D, 1024), BF16),
        ((512, D), BF16),
        ((512, D), BF16),
        ((128, LANES), BF16),
        ((256, LANES), BF16),
        ((1, 512), F32),
        ((2, TOK, TOK), F32),
        ((TOK + CHUNKS, TOK), BF16),
        ((2, SEG, PAIRS * 128), F32),
        ((2, SEG, PAIRS * 128), F32),
        ((CHUNKS, PAIRS, 128), F32),
        ((2 * PAIRS, 128), F32),
        ((TOK, 512), F32),
        ((TOK, 512), BF16),
        ((TOK, 512), F32),
        ((TOK, LANES), F32),
        ((TOK, LANES), BF16),
        ((PAIRS * CHUNKS, 128), F32),
        ((PAIRS * CHUNKS, 128), F32),
        ((PAIRS * CHUNKS, 128), F32),
        ((PAIRS * CHUNKS, 128), F32),
        ((TOK, 512), F32),
        ((TOK + WINDOW, 512), BF16),
        ((TOK, 512), F32),
        ((TOK, 512), F32),
        ((TOK, 512), BF16),
        ((TOK, 512), BF16),
        ((TOK, D), F32),
        ((N_OUT, TOK, HALF // N_OUT), BF16),
        ((N_OUT, TOK, HALF // N_OUT), BF16),
        ((plane, 1, 128), F32),
        ((plane, 2, PAIRS, 128), BF16),
        ((nz, 1, 128), F32),
        ((nz, 2, PAIRS, 128), BF16),
        ((2, PAIRS, 128), F32),
    ]
    dma = pltpu.SemaphoreType.DMA
    regular = pltpu.SemaphoreType.REGULAR
    return pl.pallas_call(
        functools.partial(kernel, sizes),
        out_shape=jax.ShapeDtypeStruct((TOK, HALF), BF16),
        in_specs=[hbm] * 19,
        out_specs=vmem,
        scratch_shapes=[pltpu.SMEM((8,), F32), pltpu.SMEM((2 * PAIRS,), F32)]
        + [pltpu.VMEM(shape, dtype) for shape, dtype in scratch]
        + [dma((19,)), dma((2,)), dma((2,)), dma((N_OUT,)), dma((N_OUT,))]
        + [dma((plane,))] * 4
        + [dma((nz,))] * 4
        + [regular] * 3,
        compiler_params=pltpu.CompilerParams(
            collective_id=0, has_side_effects=True, vmem_limit_bytes=48 * 1024 * 1024
        ),
        name="layer",
    )(
        *(
            pltpu.with_memory_space_constraint(array, pltpu.HBM)
            for array in (
                hidden,
                query_weight,
                key_weight,
                value_weight,
                head_gate_weight,
                state_in_weight,
                state_gate_weight,
                head_out_weight,
                state_out_weight,
                sink_logit,
                log_step,
                decay_real,
                decay_frequency,
                input_real.transpose(0, 2, 1),
                input_imaginary.transpose(0, 2, 1),
                output_real,
                output_imaginary,
                skip_weight.T,
                decay_shift,
            )
        )
    )


def solution(mesh):
    sizes = SP_SIZES[mesh.shape["sp"]]
    in_specs = (
        P("sp", "tp"),
        P(None, "tp"),
        P(None, "tp"),
        P(None, "tp"),
        P(None, "tp"),
        P(None, "tp"),
        P(None, "tp"),
        P("tp"),
        P("tp", None),
        P("tp", None),
        P("tp"),
        P("tp", None, None),
        P("tp", None, None),
        P("tp", None, None),
        P("tp", None, None),
        P("tp", None),
        P("tp", "sp"),
        P("tp", None),
        P("tp", None),
    )
    return jax.shard_map(
        functools.partial(on_device, sizes),
        mesh=mesh,
        in_specs=in_specs,
        out_specs=P("sp", "tp"),
        check_vma=False,
    )
```

time: 29.6 us -> 25.2 us (0.85)
  the two profiles are of different devices: /device:TPU:41 before, /device:TPU:225 now
where the time goes in v3:
time: 25.2 us
  Pallas kernels  24.4 us (97%)
  local copies, waits for them, and re-layouts  0.8 us (3%)
    pallas_call x1, Pallas kernels, on_device(): pl.pallas_call(functools.partial(kernel, sizes), out_shape=jax.ShapeDtype...  24.4 us
    unnamed x1, local copies, waits for them, and re-layouts  0.8 us

profile of v3, /device:TPU:225, one launch (start us, length us, event | category | flops | bytes accessed | tf_op | source)
XLA Modules:
  0.0 25.2 jit_solution(5213714090882787353)
XLA Ops:
  0.0 24.4 %layer.1 = bf16[256,1024]{1,0:T(8,128)(2,1)S(1)} custom-call(bf16[256,1024]{1,0:T(8,128)(2,1)} %refs_0_.1, bf16[2048,512]{1,0:T(8,128)(2,1)} %refs_1_.1, bf16[2048,256]{1,0:T(8,128)(2,1)} %refs_2_.1, bf16[2048,256]{1,0:T(8,128)(2,1)} %refs_3_.1, bf16[2048,512]{1,0:T(8,128)(2,1)} %refs_4_.1, bf16[2048,512]{1,0:T(8,128)(2,1)} %refs_5_.1, ...), custom_call_target="tpu_custom_call" | custom-call | tf_op jit(solution)/shard_map/layer/pallas_call | solution.py:664
  24.4 0.8 %copy.21 = bf16[256,1024]{1,0:T(8,128)(2,1)} copy(bf16[256,1024]{1,0:T(8,128)(2,1)S(1)} %layer.1) | data formatting | bytes 1048576

commit v4 on v3

--- a/solution.py
+++ b/solution.py
@@ -206,6 +206,19 @@
     ]
     l_in = load(w_sin, win)
 
+    row = lax.broadcasted_iota(jnp.int32, (TOK, TOK), 0)
+    col = lax.broadcasted_iota(jnp.int32, (TOK, TOK), 1)
+    tri[0:TOK, :] = ((row // SEG == col // SEG) & (col <= row)).astype(F32).astype(BF16)
+    srow = lax.broadcasted_iota(jnp.int32, (CHUNKS, TOK), 0)
+    scol = lax.broadcasted_iota(jnp.int32, (CHUNKS, TOK), 1)
+    tri[TOK:, :] = (scol // SEG == srow).astype(F32).astype(BF16)
+    drive[...] = jnp.zeros_like(drive)
+    cmat[...] = jnp.zeros_like(cmat)
+    qi = lax.rem(row, WINDOW)
+    inside = (col > qi) & (col <= qi + WINDOW)
+    bias[0] = jnp.where(inside & ((col >= WINDOW) | (sp > 0)), 0.0, -1e30)
+    bias[1] = jnp.where(inside, 0.0, -1e30)
+
     pl.semaphore_wait(barrier, 1 + count(ahead) + z + count([crosses]))
     l_h.wait()
     send_h = remote(h_ref.at[:, mine], h_ref.at[:, mine], h_sem.at[0], h_sem.at[1], (sp, other))
@@ -250,13 +263,6 @@
         (base[1] * real - less * freq) / denominator,
     )
 
-    row = lax.broadcasted_iota(jnp.int32, (TOK, TOK), 0)
-    col = lax.broadcasted_iota(jnp.int32, (TOK, TOK), 1)
-    tri[0:TOK, :] = ((row // SEG == col // SEG) & (col <= row)).astype(F32).astype(BF16)
-    srow = lax.broadcasted_iota(jnp.int32, (CHUNKS, TOK), 0)
-    scol = lax.broadcasted_iota(jnp.int32, (CHUNKS, TOK), 1)
-    tri[TOK:, :] = (scol // SEG == srow).astype(F32).astype(BF16)
-    drive[...] = jnp.zeros_like(drive)
     for i in range(PAIRS):
         factor = (zoh[0][i : i + 1, :], zoh[1][i : i + 1, :])
         first = (i % 4) * 32
@@ -266,7 +272,138 @@
             drive[first : first + 16, cols] = jnp.where(low, value[part], 0.0).astype(BF16)
             drive[first + 16 : first + 32, cols] = jnp.where(low, 0.0, value[part]).astype(BF16)
 
-    cmat[...] = jnp.zeros_like(cmat)
+    power = lax.broadcasted_iota(jnp.int32, (8, 128), 0) + 1
+    ones, zeros = jnp.ones((8, 128), F32), jnp.zeros((8, 128), F32)
+
+    def power_table(table, root):
+        for i in range(PAIRS):
+            b = tuple(jnp.broadcast_to(part[i : i + 1, :], (8, 128)) for part in root)
+            value = (ones, zeros)
+            for bit in range(4):
+                has = (power >> bit) & 1 == 1
+                value = cmul(value, (jnp.where(has, b[0], ones), jnp.where(has, b[1], zeros)))
+                if bit < 3:
+                    b = cmul(b, b)
+            cols = slice(i * 128, i * 128 + 128)
+            upper = cmul(value, b)
+            for k in (0, 1):
+                table[k, 0:8, cols] = value[k]
+                table[k, 8:16, cols] = upper[k]
+    power_table(shrink, base_inv)
+    a_seg = csquares(base, log2(SEG))
+    a_dev = csquares(a_seg, log2(CHUNKS))
+    a_plane = csquares(a_dev, log2(plane))
+
+    def shift_sums(mask):
+        rest = jnp.broadcast_to(shift[...][:, None, :], (2 * PAIRS, 16, TOK)).reshape(512, TOK)
+        sums = None
+        for _ in range(3):
+            part = rest.astype(BF16)
+            term = dot_nt(mask, part)
+            sums = term if sums is None else sums + term
+            rest = rest - part.astype(F32)
+        return sums
+
+    es_ref[...] = shift_sums(tri[0:TOK, :])
+    lane = lax.broadcasted_iota(jnp.int32, (PAIRS, 128), 1)
+    total_shift = jnp.zeros((PAIRS, 128), F32)
+    for c in range(CHUNKS):
+        if c % 8 == 0:
+            pair_tile[...] = shift[:, c * SEG : c * SEG + 128]
+            even = pair_tile[pl.ds(0, PAIRS, stride=2), :]
+            odd = pair_tile[pl.ds(1, PAIRS, stride=2), :]
+        inside = lane // SEG == c % 8
+        s = jnp.where(
+            low,
+            jnp.sum(jnp.where(inside, even, 0.0), axis=1, keepdims=True),
+            jnp.sum(jnp.where(inside, odd, 0.0), axis=1, keepdims=True),
+        )
+        total_shift = total_shift + s
+        decay[c] = jnp.exp(s)
+    s_buf[m] = jnp.sum(
+        jnp.where(lane % 64 == pair_row, total_shift, 0.0), axis=0, keepdims=True
+    )
+
+    l_in.wait()
+    u_ref[...] = dot(h_ref[:, mine], win[mine, :])
+    send_h.wait_recv()
+    l_hg = load(w_hgate, wgate.at[:, 0:512])
+    l_sg = load(w_sgate, wgate.at[:, 512:1024])
+    l_ho = load(w_hout, who)
+    l_so = load(w_sout, wso)
+    u = (u_ref[...] + dot(h_ref[:, theirs], win[theirs, :])).astype(BF16).astype(F32)
+    u_ref[...] = u
+    us_ref[...] = (u * jnp.exp(-es_ref[...])).astype(BF16)
+
+    def plane_copy(buf, send, recv, k):
+        return remote(buf.at[m], buf.at[m], send.at[k], recv.at[m], (z * plane + k, tp))
+
+    def plane_wait(buf, send, recv, k):
+        remote(buf.at[k], buf.at[k], send.at[k], recv.at[k], (z * plane + k, tp)).wait_recv()
+
+    for i in range(PAIRS):
+        cols, narrow = slice(i * 256, i * 256 + 256), slice(i * 128, i * 128 + 128)
+        j = i // 4
+        push = dot(us_ref[:, j * 128 : j * 128 + 128], drive[:, cols])
+        push = (push[:, :128].reshape(CHUNKS, SEG, 128), push[:, 128:].reshape(CHUNKS, SEG, 128))
+        back = (shrink[0, :, narrow][None], shrink[1, :, narrow][None])
+        w = cmul(push, back)
+        w = jnp.concatenate([part.reshape(TOK, 128).astype(BF16) for part in w], axis=1)
+        summed = dot(tri[...], w)
+        x_ref[:, cols] = summed[:TOK]
+        tot_re[i * 16 : i * 16 + 16, :] = summed[TOK:, :128]
+        tot_im[i * 16 : i * 16 + 16, :] = summed[TOK:, 128:]
+
+    flat_zero = jnp.zeros((PAIRS, 128), F32)
+    flat_one = jnp.ones((PAIRS, 128), F32)
+
+    def chunk_scan(state, keep):
+        for c in range(CHUNKS):
+            at = pl.ds(c, PAIRS, stride=CHUNKS)
+            if keep:
+                ent_re[at, :] = state[0]
+                ent_im[at, :] = state[1]
+            e = decay[c]
+            state = cmul(
+                (state[0] + tot_re[at, :], state[1] + tot_im[at, :]), (a_seg[0] * e, a_seg[1] * e)
+            )
+        return state
+
+    state = chunk_scan((flat_zero, flat_zero), False)
+    l_buf[m, 0] = state[0].astype(BF16)
+    l_buf[m, 1] = state[1].astype(BF16)
+    def send_to(k, condition):
+        when(condition, plane_copy(l_buf, l_send, l_recv, k).start)
+        when(condition, plane_copy(s_buf, s_send, s_recv, k).start)
+
+    near = [jnp.logical_and(behind[k], apart[k] < FAR) for k in range(plane)]
+    far = [apart[k] >= FAR for k in range(plane)]
+    for k in range(plane):
+        send_to(k, ahead[k])
+    row_end = m % nx == nx - 1
+    late = max(nz // 2 - 1, 1)
+    late_cross = jnp.logical_and(m == plane - 1, z < late)
+    late_halo = jnp.logical_and(m == 0, jnp.logical_and(z > 0, z <= late))
+    l_k.wait()
+    l_v.wait()
+    halo = remote(
+        kv_ref.at[TOK : TOK + WINDOW, :],
+        kv_ref.at[0:WINDOW, :],
+        halo_sem.at[0],
+        halo_sem.at[1],
+        (lax.rem(sp + 1, nz * plane), tp),
+    )
+
+    @pl.when(row_end)
+    def _():
+        kv_ref[TOK:, :] = dot(h_ref[WINDOW:, :], wkvq[:, 0:512]).astype(BF16)
+    when(count(near) > 0, pl.semaphore_wait, ready_near, jnp.maximum(count(near), 1))
+    for k in range(plane):
+        send_to(k, near[k])
+    early = jnp.logical_and(row_end, jnp.logical_or(m < plane - 1, z >= late))
+    pl.when(jnp.logical_and(early, sp < nz * plane - 1))(halo.start)
+
+    power_table(grow, base)
     for i in range(PAIRS):
         first = (i % 8) * 32
         value = [jnp.concatenate([t[2 * i], t[2 * i + 1]], axis=1) for t in (out_re, out_im)]
@@ -287,136 +424,6 @@
     skip_ref[...] = jnp.sum(
         jnp.where((channel % 16 == group)[:16], spread_skip, 0.0), axis=0, keepdims=True
     )
-    qi = lax.rem(row, WINDOW)
-    inside = (col > qi) & (col <= qi + WINDOW)
-    bias[0] = jnp.where(inside & ((col >= WINDOW) | (sp > 0)), 0.0, -1e30)
-    bias[1] = jnp.where(inside, 0.0, -1e30)
-
-    power = lax.broadcasted_iota(jnp.int32, (8, 128), 0) + 1
-    ones, zeros = jnp.ones((8, 128), F32), jnp.zeros((8, 128), F32)
-    for table, root in ((grow, base), (shrink, base_inv)):
-        for i in range(PAIRS):
-            b = tuple(jnp.broadcast_to(part[i : i + 1, :], (8, 128)) for part in root)
-            value = (ones, zeros)
-            for bit in range(4):
-                has = (power >> bit) & 1 == 1
-                value = cmul(value, (jnp.where(has, b[0], ones), jnp.where(has, b[1], zeros)))
-                if bit < 3:
-                    b = cmul(b, b)
-            cols = slice(i * 128, i * 128 + 128)
-            upper = cmul(value, b)
-            for k in (0, 1):
-                table[k, 0:8, cols] = value[k]
-                table[k, 8:16, cols] = upper[k]
-    a_seg = csquares(base, log2(SEG))
-    a_dev = csquares(a_seg, log2(CHUNKS))
-    a_plane = csquares(a_dev, log2(plane))
-
-    def shift_sums(mask):
-        rest = jnp.broadcast_to(shift[...][:, None, :], (2 * PAIRS, 16, TOK)).reshape(512, TOK)
-        sums = None
-        for _ in range(3):
-            part = rest.astype(BF16)
-            term = dot_nt(mask, part)
-            sums = term if sums is None else sums + term
-            rest = rest - part.astype(F32)
-        return sums
-
-    es_ref[...] = shift_sums(tri[0:TOK, :])
-    lane = lax.broadcasted_iota(jnp.int32, (PAIRS, 128), 1)
-    total_shift = jnp.zeros((PAIRS, 128), F32)
-    for c in range(CHUNKS):
-        if c % 8 == 0:
-            pair_tile[...] = shift[:, c * SEG : c * SEG + 128]
-            even = pair_tile[pl.ds(0, PAIRS, stride=2), :]
-            odd = pair_tile[pl.ds(1, PAIRS, stride=2), :]
-        inside = lane // SEG == c % 8
-        s = jnp.where(
-            low,
-            jnp.sum(jnp.where(inside, even, 0.0), axis=1, keepdims=True),
-            jnp.sum(jnp.where(inside, odd, 0.0), axis=1, keepdims=True),
-        )
-        total_shift = total_shift + s
-        decay[c] = jnp.exp(s)
-    s_buf[m] = jnp.sum(
-        jnp.where(lane % 64 == pair_row, total_shift, 0.0), axis=0, keepdims=True
-    )
-
-    l_in.wait()
-    u_ref[...] = dot(h_ref[:, mine], win[mine, :])
-    send_h.wait_recv()
-    l_hg = load(w_hgate, wgate.at[:, 0:512])
-    l_sg = load(w_sgate, wgate.at[:, 512:1024])
-    l_ho = load(w_hout, who)
-    l_so = load(w_sout, wso)
-    row_end = m % nx == nx - 1
-    l_k.wait()
-    l_v.wait()
-    halo = remote(
-        kv_ref.at[TOK : TOK + WINDOW, :],
-        kv_ref.at[0:WINDOW, :],
-        halo_sem.at[0],
-        halo_sem.at[1],
-        (lax.rem(sp + 1, nz * plane), tp),
-    )
-
-    @pl.when(row_end)
-    def _():
-        kv_ref[TOK:, :] = dot(h_ref[WINDOW:, :], wkvq[:, 0:512]).astype(BF16)
-
-    u = (u_ref[...] + dot(h_ref[:, theirs], win[theirs, :])).astype(BF16).astype(F32)
-    u_ref[...] = u
-    us_ref[...] = (u * jnp.exp(-es_ref[...])).astype(BF16)
-    pl.when(jnp.logical_and(row_end, sp < nz * plane - 1))(halo.start)
-
-    def plane_copy(buf, send, recv, k):
-        return remote(buf.at[m], buf.at[m], send.at[k], recv.at[m], (z * plane + k, tp))
-
-    def plane_wait(buf, send, recv, k):
-        remote(buf.at[k], buf.at[k], send.at[k], recv.at[k], (z * plane + k, tp)).wait_recv()
-
-    for i in range(PAIRS):
-        cols, narrow = slice(i * 256, i * 256 + 256), slice(i * 128, i * 128 + 128)
-        j = i // 4
-        push = dot(us_ref[:, j * 128 : j * 128 + 128], drive[:, cols])
-        push = (push[:, :128].reshape(CHUNKS, SEG, 128), push[:, 128:].reshape(CHUNKS, SEG, 128))
-        back = (shrink[0, :, narrow][None], shrink[1, :, narrow][None])
-        w = cmul(push, back)
-        w = jnp.concatenate([part.reshape(TOK, 128).astype(BF16) for part in w], axis=1)
-        summed = dot(tri[...], w)
-        x_ref[:, cols] = summed[:TOK]
-        tot_re[i * 16 : i * 16 + 16, :] = summed[TOK:, :128]
-        tot_im[i * 16 : i * 16 + 16, :] = summed[TOK:, 128:]
-
-    flat_zero = jnp.zeros((PAIRS, 128), F32)
-    flat_one = jnp.ones((PAIRS, 128), F32)
-
-    def chunk_scan(state, keep):
-        for c in range(CHUNKS):
-            at = pl.ds(c, PAIRS, stride=CHUNKS)
-            if keep:
-                ent_re[at, :] = state[0]
-                ent_im[at, :] = state[1]
-            e = decay[c]
-            state = cmul(
-                (state[0] + tot_re[at, :], state[1] + tot_im[at, :]), (a_seg[0] * e, a_seg[1] * e)
-            )
-        return state
-
-    state = chunk_scan((flat_zero, flat_zero), False)
-    l_buf[m, 0] = state[0].astype(BF16)
-    l_buf[m, 1] = state[1].astype(BF16)
-    def send_to(k, condition):
-        when(condition, plane_copy(l_buf, l_send, l_recv, k).start)
-        when(condition, plane_copy(s_buf, s_send, s_recv, k).start)
-
-    near = [jnp.logical_and(behind[k], apart[k] < FAR) for k in range(plane)]
-    far = [apart[k] >= FAR for k in range(plane)]
-    for k in range(plane):
-        send_to(k, ahead[k])
-    when(count(near) > 0, pl.semaphore_wait, ready_near, jnp.maximum(count(near), 1))
-    for k in range(plane):
-        send_to(k, near[k])
 
     l_q.wait()
     rows = dot(h_ref[...], wkvq[...]).astype(BF16)
@@ -437,6 +444,8 @@
     gates = jax.nn.sigmoid(dot(h_ref[...], wgate[...]).astype(BF16).astype(F32))
     hg_ref[...] = gates[:, 0:512]
     sg_ref[...] = gates[:, 512:1024]
+
+    pl.when(late_cross)(halo.start)
 
     left = lax.broadcasted_iota(jnp.int32, (WINDOW, 128), 1) < 64
 
@@ -513,13 +522,16 @@
 
     l_ho.wait()
 
-    @pl.when(sp == 0)
-    def _():
-        kv_ref[0:WINDOW, :] = jnp.zeros((WINDOW, 512), BF16)
-
-    pl.when(sp > 0)(halo.wait_recv)
-    attend(0)
-    acc_ref[...] = dot(hm_ref[...], who[...])
+    def finish_heads():
+        @pl.when(sp == 0)
+        def _():
+            kv_ref[0:WINDOW, :] = jnp.zeros((WINDOW, 512), BF16)
+
+        pl.when(sp > 0)(halo.wait_recv)
+        attend(0)
+        acc_ref[...] = dot(hm_ref[...], who[...])
+
+    pl.when(jnp.logical_not(late_halo))(finish_heads)
 
     pre[...] = jnp.zeros_like(pre)
     for k in range(nz - 1):
@@ -557,6 +569,8 @@
         rec = dot_nt(s_ref[:, wide], cmat[:, wide])
         rec = rec * jnp.exp(es_ref[:, cols]) + skip_ref[:, cols] * u_ref[:, cols]
         sm_ref[:, cols] = (sg_ref[:, cols] * jax.nn.gelu(rec)).astype(BF16)
+
+    pl.when(late_halo)(finish_heads)
 
     l_so.wait()
     outs = []

time: 25.2 us -> 23.9 us (0.948); the launches traced: 25.2 us -> 23.5 us
  Pallas kernels: 24.4 us -> 22.7 us
    pallas_call x1, Pallas kernels: 24.4 us -> 22.7 us  [on_device(): pl.pallas_call(functools.partial(kernel, sizes), out_shape=jax.ShapeDtype...]
where the time goes in v4:
time: 23.9 us; the launch traced here: 23.5 us
  Pallas kernels  22.7 us (95%)
  local copies, waits for them, and re-layouts  0.8 us (3%)
    pallas_call x1, Pallas kernels, on_device(): pl.pallas_call(functools.partial(kernel, sizes), out_shape=jax.ShapeDtype...  22.7 us
    unnamed x1, local copies, waits for them, and re-layouts  0.8 us

profile of v4, /device:TPU:225, one launch (start us, length us, event | category | flops | bytes accessed | tf_op | source)
XLA Modules:
  0.0 23.5 jit_solution(17697252855044384762)
XLA Ops:
  0.0 22.7 %layer.1 = bf16[256,1024]{1,0:T(8,128)(2,1)S(1)} custom-call(bf16[256,1024]{1,0:T(8,128)(2,1)} %refs_0_.1, bf16[2048,512]{1,0:T(8,128)(2,1)} %refs_1_.1, bf16[2048,256]{1,0:T(8,128)(2,1)} %refs_2_.1, bf16[2048,256]{1,0:T(8,128)(2,1)} %refs_3_.1, bf16[2048,512]{1,0:T(8,128)(2,1)} %refs_4_.1, bf16[2048,512]{1,0:T(8,128)(2,1)} %refs_5_.1, ...), custom_call_target="tpu_custom_call" | custom-call | tf_op jit(solution)/shard_map/layer/pallas_call | solution.py:678
  22.7 0.8 %copy.21 = bf16[256,1024]{1,0:T(8,128)(2,1)} copy(bf16[256,1024]{1,0:T(8,128)(2,1)S(1)} %layer.1) | data formatting | bytes 1048576

commit v5 on v4

--- a/solution.py
+++ b/solution.py
@@ -381,7 +381,7 @@
     for k in range(plane):
         send_to(k, ahead[k])
     row_end = m % nx == nx - 1
-    late = max(nz // 2 - 1, 1)
+    late = nz - 1
     late_cross = jnp.logical_and(m == plane - 1, z < late)
     late_halo = jnp.logical_and(m == 0, jnp.logical_and(z > 0, z <= late))
     l_k.wait()

time: 23.9 us -> 25 us (1.046)
  the two profiles are of different devices: /device:TPU:225 before, /device:TPU:129 now
where the time goes in v5:
time: 25 us; the launch traced here: 24.9 us
  Pallas kernels  24.1 us (96%)
  local copies, waits for them, and re-layouts  0.8 us (3%)
    pallas_call x1, Pallas kernels, on_device(): pl.pallas_call(functools.partial(kernel, sizes), out_shape=jax.ShapeDtype...  24.1 us
    unnamed x1, local copies, waits for them, and re-layouts  0.8 us

profile of v5, /device:TPU:129, one launch (start us, length us, event | category | flops | bytes accessed | tf_op | source)
XLA Modules:
  0.0 24.9 jit_solution(14835322473013538684)
XLA Ops:
  0.0 24.1 %layer.1 = bf16[256,1024]{1,0:T(8,128)(2,1)S(1)} custom-call(bf16[256,1024]{1,0:T(8,128)(2,1)} %refs_0_.1, bf16[2048,512]{1,0:T(8,128)(2,1)} %refs_1_.1, bf16[2048,256]{1,0:T(8,128)(2,1)} %refs_2_.1, bf16[2048,256]{1,0:T(8,128)(2,1)} %refs_3_.1, bf16[2048,512]{1,0:T(8,128)(2,1)} %refs_4_.1, bf16[2048,512]{1,0:T(8,128)(2,1)} %refs_5_.1, ...), custom_call_target="tpu_custom_call" | custom-call | tf_op jit(solution)/shard_map/layer/pallas_call | solution.py:678
  24.1 0.8 %copy.21 = bf16[256,1024]{1,0:T(8,128)(2,1)} copy(bf16[256,1024]{1,0:T(8,128)(2,1)S(1)} %layer.1) | data formatting | bytes 1048576

commit v6 on v4

--- a/solution.py
+++ b/solution.py
@@ -400,8 +400,7 @@
     when(count(near) > 0, pl.semaphore_wait, ready_near, jnp.maximum(count(near), 1))
     for k in range(plane):
         send_to(k, near[k])
-    early = jnp.logical_and(row_end, jnp.logical_or(m < plane - 1, z >= late))
-    pl.when(jnp.logical_and(early, sp < nz * plane - 1))(halo.start)
+    pl.when(jnp.logical_and(row_end, m < plane - 1))(halo.start)
 
     power_table(grow, base)
     for i in range(PAIRS):
@@ -434,7 +433,8 @@
     def _():
         kv_ref[TOK:, :] = rows[WINDOW:, 0:512]
 
-    pl.when(jnp.logical_not(row_end))(halo.start)
+    soon = jnp.logical_and(crosses, z >= late)
+    pl.when(jnp.logical_or(jnp.logical_not(row_end), soon))(halo.start)
     when(count(far) > 0, pl.semaphore_wait, ready_far, jnp.maximum(count(far), 1))
     for k in range(plane):
         send_to(k, far[k])

time: 23.9 us -> 24.8 us (1.038); the launches traced: 23.5 us -> 24.8 us
  Pallas kernels: 22.7 us -> 23.9 us
    pallas_call x1, Pallas kernels: 22.7 us -> 23.9 us  [on_device(): pl.pallas_call(functools.partial(kernel, sizes), out_shape=jax.ShapeDtype...]
where the time goes in v6:
time: 24.8 us
  Pallas kernels  23.9 us (96%)
  local copies, waits for them, and re-layouts  0.8 us (3%)
    pallas_call x1, Pallas kernels, on_device(): pl.pallas_call(functools.partial(kernel, sizes), out_shape=jax.ShapeDtype...  23.9 us
    unnamed x1, local copies, waits for them, and re-layouts  0.8 us

profile of v6, /device:TPU:225, one launch (start us, length us, event | category | flops | bytes accessed | tf_op | source)
XLA Modules:
  0.0 24.8 jit_solution(9291457079382585633)
XLA Ops:
  0.0 23.9 %layer.1 = bf16[256,1024]{1,0:T(8,128)(2,1)S(1)} custom-call(bf16[256,1024]{1,0:T(8,128)(2,1)} %refs_0_.1, bf16[2048,512]{1,0:T(8,128)(2,1)} %refs_1_.1, bf16[2048,256]{1,0:T(8,128)(2,1)} %refs_2_.1, bf16[2048,256]{1,0:T(8,128)(2,1)} %refs_3_.1, bf16[2048,512]{1,0:T(8,128)(2,1)} %refs_4_.1, bf16[2048,512]{1,0:T(8,128)(2,1)} %refs_5_.1, ...), custom_call_target="tpu_custom_call" | custom-call | tf_op jit(solution)/shard_map/layer/pallas_call | solution.py:678
  24.0 0.8 %copy.21 = bf16[256,1024]{1,0:T(8,128)(2,1)} copy(bf16[256,1024]{1,0:T(8,128)(2,1)S(1)} %layer.1) | data formatting | bytes 1048576
